TPU v7x, 768 devices: a whole 4x8x12 slice. The times are simulated.
768 devices in a mesh: ep: 48 (over z, x), tp: 16 (over y, core).
Axes of the slice: x: 4, y: 8, z: 12, core: 2. Of those that a mesh axis runs over, the one named last changes fastest.
Arguments:
- tokens: bfloat16 [6144, 2048], P('ep'), may hold values from -6 to 6
- routes: int32 [6144, 2], P('ep'), may hold values from 0 to 47, all different within a row; in each aligned block of 128 rows (0 to 127, 128 to 255, ...) at most 6 rows name the same one
- route_gates: float32 [6144, 2], P('ep'), may hold values from 0.1 to 2
- cotangent: bfloat16 [6144, 2048], P('ep'), may hold values from -40 to 40
- w_gate: bfloat16 [48, 2048, 1536], P('ep', None, 'tp'), may hold values from -0.125 to 0.125
- w_up: bfloat16 [48, 2048, 1536], P('ep', None, 'tp'), may hold values from -0.125 to 0.125
- w_down: bfloat16 [48, 1536, 2048], P('ep', 'tp'), may hold values from -0.15625 to 0.15625
- s_gate: bfloat16 [2048, 1536], P(None, 'tp'), may hold values from -0.125 to 0.125
- s_up: bfloat16 [2048, 1536], P(None, 'tp'), may hold values from -0.125 to 0.125
- s_down: bfloat16 [1536, 2048], P('tp'), may hold values from -0.15625 to 0.15625
Outputs:
- token_grad: bfloat16 [6144, 2048], P('ep', 'tp')
- gate_grad: float32 [6144, 2], P('ep')
- grad_gate: float32 [48, 2048, 1536], P('ep', None, 'tp')
- grad_up: float32 [48, 2048, 1536], P('ep', None, 'tp')
- grad_down: float32 [48, 1536, 2048], P('ep', 'tp')
- grad_shared: float32 [1536, 2048], P(('tp', 'ep'))
- norm_in: float32 [48, 2, 2048], P('ep')
- norm_down: float32 [48, 1536], P('ep', 'tp')
- norm_shared: float32 [1536], P(('tp', 'ep'))
Inputs may be any that keep to these rules, and one draw needn't show every extreme that they name: `routes`: within the rows of one index of ep no expert is named by more than 6 assignments, a bound that some block reaches.
All inputs are finite; a program needn't handle non-finite values.
Results may differ from a plain program's by a relative error of at most 0.0095.
Values may be sent and summed in bfloat16 or wider, within the bound.
No kernel may reach another device: no remote copies, remote signals or barrier semaphores. Data moves between devices by JAX's collectives and lax.ppermute only.
A program may use at most 64 MiB of HBM per device.

v0:
```python
import math

import jax
import jax.numpy as jnp
from jax import lax
from jax.sharding import PartitionSpec as P


def in_blocks(x, dim, peers):
    lengths = x.shape
    tiles = x.reshape(*lengths[:dim], peers, lengths[dim] // peers, *lengths[dim + 1 :])
    return jnp.moveaxis(tiles, dim, 0)


def sent_and_summed(x, axis, dim):
    peers = lax.axis_size(axis)
    tiles = lax.all_to_all(in_blocks(x, dim, peers), axis, 0, 0, tiled=True)
    return jnp.sum(tiles, axis=0)


def side_by_side(arrays, axis, split_dim, concat_dim, along):
    widths = [a.shape[along] for a in arrays]
    both = jnp.concatenate(arrays, axis=along)
    whole = lax.all_to_all(both, axis, split_axis=split_dim, concat_axis=concat_dim, tiled=True)
    return tuple(jnp.split(whole, [sum(widths[:k]) for k in range(1, len(widths))], axis=along))


def side_by_side_2(arrays, axis, dim, along):
    both = jnp.concatenate(arrays, axis=along)
    whole, at, done = (lax.all_gather(both, axis, axis=dim, tiled=True), 0, [])
    for a in arrays:
        done.append(lax.slice_in_dim(whole, at, at + a.shape[along], axis=along))
        at += a.shape[along]
    return tuple(done)


def sent_to_all(x, axis):
    copies = jnp.broadcast_to(x, (lax.axis_size(axis), *x.shape))
    return lax.all_to_all(copies, axis, split_axis=0, concat_axis=0, tiled=True)


def taken_together(x, axis):
    everything = sent_to_all(x, axis)
    return jnp.sum(everything, axis=0)


def packed_total(arrays, axis):
    line, at, done = (jnp.concatenate([a.reshape(-1) for a in arrays]), 0, [])
    subtotal = taken_together(line, axis)
    for a in arrays:
        done.append(subtotal[at : at + a.size].reshape(a.shape))
        at += a.size
    return tuple(done)


def in_one_piece(arrays, axis, split_dim, concat_dim, along):
    widths = [math.prod(a.shape[along:]) for a in arrays]
    both = jnp.concatenate(
        [a.reshape(*a.shape[:along], w) for a, w in zip(arrays, widths)], axis=along
    )
    whole = lax.all_to_all(both, axis, split_axis=split_dim, concat_axis=concat_dim, tiled=True)
    tiles = jnp.split(whole, [sum(widths[:k]) for k in range(1, len(widths))], axis=along)
    return tuple((b.reshape(*whole.shape[:along], *a.shape[along:]) for a, b in zip(arrays, tiles)))


def swiglu_back(rows_x, rows_c, gate_weight, up_weight, down_weight):
    pre_gate = jnp.dot(rows_x, gate_weight, preferred_element_type=jnp.float32)
    pre_up = jnp.dot(rows_x, up_weight, preferred_element_type=jnp.float32)
    sigmoid_gate = jax.nn.sigmoid(pre_gate)
    activated = pre_gate * sigmoid_gate
    hidden = (activated * pre_up).astype(jnp.bfloat16)
    hidden_grad = jnp.einsum("rd,fd->rf", rows_c, down_weight, preferred_element_type=jnp.float32)
    d_gate = (hidden_grad * pre_up * sigmoid_gate * (1.0 + pre_gate * (1.0 - sigmoid_gate))).astype(
        jnp.bfloat16
    )
    d_up = (hidden_grad * activated).astype(jnp.bfloat16)
    joined_grad = jnp.concatenate([d_gate, d_up], axis=1)
    joined_weight = jnp.concatenate([gate_weight, up_weight], axis=1)
    back_rows = jnp.einsum(
        "rf,df->rd", joined_grad, joined_weight, preferred_element_type=jnp.float32
    )
    return (hidden, hidden_grad, d_gate, d_up, back_rows.astype(jnp.bfloat16))


def reduce_shared(shared_term):
    return sent_and_summed(shared_term, "ep", 0)


def on_device(tokens, routes, route_gates, cotangent, w_gate, w_up, w_down, s_gate, s_up, s_down):
    ep_count = lax.axis_size("ep")
    tp_count = lax.axis_size("tp")
    tok_count, model_width = tokens.shape
    top_count = routes.shape[1]
    capacity = max(2, (9 * tok_count * top_count + 8 * ep_count - 1) // (8 * ep_count))
    feature_share = model_width // tp_count
    s_hidden, s_hidden_grad, s_d_gate, s_d_up, shared_piece = swiglu_back(
        tokens, cotangent, s_gate, s_up, s_down
    )
    shared_term = jnp.einsum("ts,td->sd", s_hidden, cotangent, preferred_element_type=jnp.float32)
    chosen = routes.reshape(tok_count * top_count)
    expert_ids = jnp.arange(ep_count, dtype=jnp.int32)
    one_hot = (chosen[:, None] == expert_ids[None, :]).astype(jnp.int32)
    ranks = jnp.sum((jnp.cumsum(one_hot, axis=0) - one_hot) * one_hot, axis=1)
    slot_of = chosen * capacity + ranks
    token_of = jnp.arange(tok_count * top_count, dtype=jnp.int32) // top_count
    row_token = jnp.full((ep_count * capacity,), tok_count, jnp.int32).at[slot_of].set(token_of)
    row_gate = (
        jnp.zeros((ep_count * capacity,), jnp.float32)
        .at[slot_of]
        .set(route_gates.reshape(tok_count * top_count))
    )
    padded_x = jnp.concatenate([tokens, jnp.zeros((1, model_width), jnp.bfloat16)], axis=0)
    padded_c = jnp.concatenate([cotangent, jnp.zeros((1, model_width), jnp.bfloat16)], axis=0)
    send_x = padded_x[row_token].reshape(ep_count, capacity, model_width)
    send_c = (row_gate[:, None] * padded_c[row_token].astype(jnp.float32)).astype(jnp.bfloat16)
    send_c = send_c.reshape(ep_count, capacity, model_width)
    start = lax.axis_index("tp") * feature_share
    part_x = lax.dynamic_slice_in_dim(send_x, start, feature_share, 2)
    part_c = lax.dynamic_slice_in_dim(send_c, start, feature_share, 2)
    moved_x, moved_c = side_by_side((part_x, part_c), "ep", 0, 0, 1)
    recv_x, recv_c = side_by_side_2((moved_x, moved_c), "tp", 2, 0)
    rows_x = recv_x.reshape(ep_count * capacity, model_width)
    rows_c = recv_c.reshape(ep_count * capacity, model_width)
    hidden, hidden_grad, d_gate, d_up, slot_part = swiglu_back(
        rows_x, rows_c, w_gate[0], w_up[0], w_down[0]
    )
    gate_part = jnp.sum(hidden.astype(jnp.float32) * hidden_grad, axis=1)
    g_gate = jnp.einsum("rd,rf->df", rows_x, d_gate, preferred_element_type=jnp.float32)
    g_up = jnp.einsum("rd,rf->df", rows_x, d_up, preferred_element_type=jnp.float32)
    g_down = jnp.einsum("rf,rd->fd", hidden, rows_c, preferred_element_type=jnp.float32)
    square_part = jnp.stack([jnp.sum(g_gate**2, axis=1), jnp.sum(g_up**2, axis=1)], axis=0)
    gate_total, square_total = packed_total((gate_part, square_part), "tp")
    ff_total = tp_count * w_gate.shape[2]
    norm_in = (square_total / ff_total)[None]
    gate_rounded = gate_total.astype(jnp.bfloat16)
    slot_parts, shared_parts = side_by_side((slot_part[None], shared_piece[None]), "tp", 2, 0, 1)
    slot_sum = jnp.sum(slot_parts.astype(jnp.float32), axis=0)
    shared_back = jnp.sum(shared_parts.astype(jnp.float32), axis=0)
    back_rows, back_dots = in_one_piece(
        (
            slot_sum.reshape(ep_count, capacity, feature_share),
            gate_rounded.astype(jnp.float32).reshape(ep_count, capacity),
        ),
        "ep",
        0,
        0,
        2,
    )
    picked = back_rows.reshape(ep_count * capacity, feature_share)[slot_of].reshape(
        tok_count, top_count, feature_share
    )
    token_grad = (jnp.sum(picked, axis=1) + shared_back).astype(jnp.bfloat16)
    gate_grad = (
        back_dots.reshape(ep_count * capacity)[slot_of].reshape(tok_count, top_count) / route_gates
    )
    grad_shared = reduce_shared(shared_term)
    norm_shared = jnp.mean(grad_shared**2, axis=1)
    norm_down = jnp.mean(g_down**2, axis=1)[None]
    return (
        token_grad,
        gate_grad,
        g_gate[None],
        g_up[None],
        g_down[None],
        grad_shared,
        norm_in,
        norm_down,
        norm_shared,
    )


def solution(mesh):
    placed = (
        P("ep", None),
        P("ep", None),
        P("ep", None),
        P("ep", None),
        P("ep", None, "tp"),
        P("ep", None, "tp"),
        P("ep", "tp", None),
        P(None, "tp"),
        P(None, "tp"),
        P("tp", None),
    )
    return jax.shard_map(
        on_device,
        mesh=mesh,
        in_specs=placed,
        out_specs=(
            P("ep", "tp"),
            P("ep", None),
            P("ep", None, "tp"),
            P("ep", None, "tp"),
            P("ep", "tp", None),
            P(("tp", "ep"), None),
            P("ep", None, None),
            P("ep", "tp"),
            P(("tp", "ep")),
        ),
        check_vma=False,
    )
```

profile of v0, /device:TPU:1, one launch (start us, length us, event | category | flops | bytes accessed | tf_op | source)
XLA Modules:
  0.0 262.2 jit_solution(4179256275619461584)
XLA Ops:
  7.3 0.8 broadcast_multiply_fusion
  8.0 0.8 copy.57
  9.4 0.8 copy.60
  10.3 0.6 reduce-window.6
  11.3 1.4 scatter_custom_fusion
  12.7 1.4 scatter_custom_fusion.1
  14.2 1.1 concatenate.33
  15.4 2.4 gather_fusion.1
  17.8 3.0 %gather_fusion = bf16[288,2048]{1,0:T(8,128)(2,1)} fusion(bf16[129,2048]{1,0:T(8,128)(2,1)S(1)} %concatenate.33, s32[1024]{0:T(1024)S(1)} %pad_clamp_fusion.1), kind=kCustom, calls=%fused_computation | custom fusion | bytes 2360448 | tf_op jit(solution)/shard_map/gather | solution.py:114
  20.8 3.1 %reshape.147 = bf16[48,6,2048]{2,1,0:T(8,128)(2,1)} reshape(bf16[288,2048]{1,0:T(8,128)(2,1)} %gather_fusion) | data formatting | bytes 2359296 | tf_op jit(solution)/shard_map/reshape | solution.py:114
  23.9 1.8 reshape.157
  25.8 1.0 constant_dynamic-slice_fusion
  26.8 1.1 fusion.10
  28.0 32.7 %all_to_all.39 = bf16[48,12,128]{2,1,0:T(8,128)(2,1)S(1)} all-to-all(bf16[48,12,128]{2,1,0:T(8,128)(2,1)S(1)} %pad_maximum_fusion.2), channel_id=1, replica_groups=mesh['ep'=48,'tp'=16] {'ep'}, dimensions={0} | all-to-all | bytes 294912 | tf_op jit(solution)/shard_map/all_to_all | solution.py:24
  60.7 0.7 pad_maximum_fusion.3
  62.1 0.9 multiply_convert_fusion.5
  63.3 1.3 reshape.156
  64.7 6.2 %all-to-all-start.4 = ((f32[48,2,2048]{2,1,0:T(2,128)}), f32[48,2,2048]{2,1,0:T(2,128)}, u32[]{:S(2)}, u32[]{:S(2)}) async-start(f32[48,2,2048]{2,1,0:T(2,128)} %reshape.156), calls=%async_computation.4 | async-start | bytes 1572864 | tf_op jit(solution)/shard_map/all_to_all | solution.py:17
  70.9 36.4 %all-gather.2.cloned.1.call-done = bf16[96,6,2048]{2,1,0:T(8,128)(2,1)} async-done(((bf16[96,6,128]{2,1,0:T(8,128)(2,1)}), bf16[96,6,2048]{2,1,0:T(8,128)(2,1)}) %all-gather.2.cloned.1.call-update) | async-done | bytes 2359312 | tf_op jit(solution)/shard_map/all_gather | solution.py:30
  107.3 3.3 %fusion.37 = (bf16[48,6,2048]{2,1,0:T(8,128)(2,1)}, bf16[48,6,2048]{2,1,0:T(8,128)(2,1)S(1)}) fusion(bf16[96,6,2048]{2,1,0:T(8,128)(2,1)} %all-gather.2.cloned.1.call-done), kind=kLoop, calls=%fused_computation.88 | loop fusion | bytes 4718592 | tf_op jit(solution)/shard_map/slice | solution.py:32
  110.6 2.3 reshape.150
  113.0 1.2 reshape.149
  114.2 1.7 fusion.32
  115.9 0.6 fusion.34
  116.5 1.2 multiply_reduce_fusion.3
  117.7 1.3 multiply_reduce_fusion.2
  119.0 1.3 multiply_reduce_fusion.1
  120.4 0.9 broadcast_in_dim.41
  121.3 5.1 %all-to-all-start.2 = ((f32[16,1,4384]{2,1,0:T(1,128)}), f32[16,1,4384]{2,1,0:T(1,128)}, u32[]{:S(2)}, u32[]{:S(2)}) async-start(f32[16,1,4384]{2,1,0:T(1,128)} %broadcast_in_dim.41), calls=%async_computation.2 | async-start | bytes 573440 | tf_op jit(solution)/shard_map/all_to_all | solution.py:39
  127.4 7.5 %copy.61 = bf16[1,416,2048]{1,0,2:T(2,128)(2,1)} copy(bf16[1,416,2048]{2,1,0:T(8,128)(2,1)S(1)} %pad_maximum_fusion) | data formatting | bytes 3407872 | tf_op jit(solution)/shard_map/concatenate | solution.py:23
  135.5 14.1 %reduce.5 = bf16[2048,416]{1,0:T(8,128)(2,1)S(1)} reduce(bf16[2048,1,416]{2,1,0:T(2,128)(2,1)} %bitcast.77, bf16[]{:T(256)} %broadcast.145), dimensions={1}, to_apply=%bitcast.53.reduce_sub_computation | reduce | bytes 3407874
  149.6 3.9 %reshape.216 = bf16[16,2,26624]{2,1,0:T(2,128)(2,1)} reshape(bf16[2048,416]{1,0:T(8,128)(2,1)S(1)} %reduce.5) | data formatting | bytes 3407872
  153.5 7.3 %all-to-all-start.1 = ((bf16[16,2,26624]{2,1,0:T(2,128)(2,1)}), bf16[16,2,26624]{2,1,0:T(2,128)(2,1)S(1)}, u32[]{:S(2)}, u32[]{:S(2)}) async-start(bf16[16,2,26624]{2,1,0:T(2,128)(2,1)} %reshape.216), calls=%async_computation.1 | async-start | bytes 3407872 | tf_op jit(solution)/shard_map/all_to_all | solution.py:24
  160.9 1.4 reduce_sum.110
  162.9 1.4 multiply_reduce_fusion
  164.3 1.2 reduce_sum.107
  165.7 36.3 %all-to-all-done.1 = bf16[16,2,26624]{2,1,0:T(2,128)(2,1)S(1)} async-done(((bf16[16,2,26624]{2,1,0:T(2,128)(2,1)}), bf16[16,2,26624]{2,1,0:T(2,128)(2,1)S(1)}, u32[]{:S(2)}, u32[]{:S(2)}) %all-to-all-start.1) | async-done | bytes 1703968 | tf_op jit(solution)/shard_map/all_to_all | solution.py:24
  202.0 8.2 %reshape.217 = bf16[2048,1,416]{2,1,0:T(2,128)(2,1)} reshape(bf16[16,2,26624]{2,1,0:T(2,128)(2,1)S(1)} %all-to-all-done.1) | data formatting | bytes 3407872
  210.2 9.2 %copy.62 = bf16[1,416,2048]{2,1,0:T(8,128)(2,1)S(1)} copy(bf16[1,416,2048]{1,0,2:T(2,128)(2,1)} %bitcast.78) | data formatting | bytes 3407872 | tf_op jit(solution)/shard_map/all_to_all | solution.py:24
  220.8 1.0 reshape.218
  221.8 13.0 %all-to-all-start.3 = ((f32[48,1,774]{2,1,0:T(1,128)}), f32[48,1,774]{2,1,0:T(1,128)S(1)}, u32[]{:S(2)}, u32[]{:S(2)}) async-start(f32[48,1,774]{2,1,0:T(1,128)} %reshape.218), calls=%async_computation.3 | async-start | bytes 344064 | tf_op jit(solution)/shard_map/all_to_all | solution.py:61
  235.4 0.6 div.40
  236.2 12.7 %all-to-all-done.3 = f32[48,1,774]{2,1,0:T(1,128)S(1)} async-done(((f32[48,1,774]{2,1,0:T(1,128)}), f32[48,1,774]{2,1,0:T(1,128)S(1)}, u32[]{:S(2)}, u32[]{:S(2)}) %all-to-all-start.3) | async-done | bytes 148640 | tf_op jit(solution)/shard_map/all_to_all | solution.py:61
  249.5 1.0 reduce.6
  251.0 0.7 gather_fusion.2
  251.8 1.9 gather_fusion.3
  254.1 0.6 copy.66
  254.7 0.6 add_convert_fusion
  (90 shorter events, 8.2 us)
Async XLA Ops:
  7.2 109.3 %copy-start = (bf16[1,96,2048]{2,1,0:T(8,128)(2,1)S(1)}, bf16[1,96,2048]{2,1,0:T(8,128)(2,1)}, u32[]{:S(2)}) copy-start(bf16[1,96,2048]{2,1,0:T(8,128)(2,1)} %param.16) | copy-start | bytes 1179652
  7.2 8.1 %copy-start.4 = (bf16[128,2048]{1,0:T(8,128)(2,1)S(1)}, bf16[128,2048]{1,0:T(8,128)(2,1)}, u32[]{:S(2)}) copy-start(bf16[128,2048]{1,0:T(8,128)(2,1)} %param.13) | copy-start | bytes 1572868
  7.2 100.1 %all-gather.2.cloned.1.call-start = ((), (), s32[]{:S(2)}) async-start(), calls=%async_computation.5 | async-start | bytes 3342336 | tf_op jit(solution)/shard_map/all_gather | solution.py:30
  10.1 3.9 %copy-start.11 = (f32[128,2]{1,0:T(8,128)}, f32[128,2]{1,0:T(8,128)S(1)}, u32[]{:S(2)}) copy-start(f32[128,2]{1,0:T(8,128)S(1)} %copy.60) | copy-start | bytes 3076
  25.8 35.7 %copy-start.3 = (bf16[128,2048]{1,0:T(8,128)(2,1)S(1)}, bf16[128,2048]{1,0:T(8,128)(2,1)}, u32[]{:S(2)}) copy-start(bf16[128,2048]{1,0:T(8,128)(2,1)} %param.10) | copy-start | bytes 1572868
  25.8 35.7 %copy-start.9 = (bf16[2048,96]{0,1:T(8,128)(2,1)S(1)}, bf16[2048,96]{0,1:T(8,128)(2,1)}, u32[]{:S(2)}) copy-start(bf16[2048,96]{0,1:T(8,128)(2,1)} %param.18) | copy-start | bytes 1179652
  26.8 35.0 %copy-start.13 = (bf16[96,2048]{1,0:T(8,128)(2,1)S(1)}, bf16[96,2048]{1,0:T(8,128)(2,1)}, u32[]{:S(2)}) copy-start(bf16[96,2048]{1,0:T(8,128)(2,1)} %param.19) | copy-start | bytes 1179652
  27.9 34.2 %copy-start.7 = (bf16[2048,96]{0,1:T(8,128)(2,1)S(1)}, bf16[2048,96]{0,1:T(8,128)(2,1)}, u32[]{:S(2)}) copy-start(bf16[2048,96]{0,1:T(8,128)(2,1)} %param.17) | copy-start | bytes 1179652
  64.7 55.7 %all-to-all-start.4 = ((f32[48,2,2048]{2,1,0:T(2,128)}), f32[48,2,2048]{2,1,0:T(2,128)}, u32[]{:S(2)}, u32[]{:S(2)}) async-start(f32[48,2,2048]{2,1,0:T(2,128)} %reshape.156), calls=%async_computation.4 | async-start | bytes 1572864 | tf_op jit(solution)/shard_map/all_to_all | solution.py:17
  112.9 2.9 %copy-start.5 = (bf16[1,2048,96]{1,2,0:T(8,128)(2,1)S(1)}, bf16[1,2048,96]{1,2,0:T(8,128)(2,1)}, u32[]{:S(2)}) copy-start(bf16[1,2048,96]{1,2,0:T(8,128)(2,1)} %param.15) | copy-start | bytes 1179652
  114.2 2.3 copy-start.1
  119.0 7.4 %copy-start.8 = (bf16[2048,96]{0,1:T(8,128)(2,1)S(1)}, bf16[2048,96]{0,1:T(8,128)(2,1)}, u32[]{:S(2)}) copy-start(bf16[2048,96]{0,1:T(8,128)(2,1)} %param.17) | copy-start | bytes 1179652
  119.0 7.4 %copy-start.10 = (bf16[2048,96]{0,1:T(8,128)(2,1)S(1)}, bf16[2048,96]{0,1:T(8,128)(2,1)}, u32[]{:S(2)}) copy-start(bf16[2048,96]{0,1:T(8,128)(2,1)} %param.18) | copy-start | bytes 1179652
  119.0 7.4 %copy-start.14 = (bf16[128,96]{0,1:T(8,128)(2,1)S(1)}, bf16[128,96]{0,1:T(8,128)(2,1)}, u32[]{:S(2)}) copy-start(bf16[128,96]{0,1:T(8,128)(2,1)} %get-tuple-element.62) | copy-start | bytes 73732
  119.0 7.5 %copy-start.15 = (bf16[128,96]{0,1:T(8,128)(2,1)S(1)}, bf16[128,96]{0,1:T(8,128)(2,1)}, u32[]{:S(2)}) copy-start(bf16[128,96]{0,1:T(8,128)(2,1)} %get-tuple-element.63) | copy-start | bytes 73732
  120.3 6.5 %copy-start.6 = (bf16[1,2048,96]{1,2,0:T(8,128)(2,1)S(1)}, bf16[1,2048,96]{1,2,0:T(8,128)(2,1)}, u32[]{:S(2)}) copy-start(bf16[1,2048,96]{1,2,0:T(8,128)(2,1)} %param.14) | copy-start | bytes 1179652
  121.3 32.2 %all-to-all-start.2 = ((f32[16,1,4384]{2,1,0:T(1,128)}), f32[16,1,4384]{2,1,0:T(1,128)}, u32[]{:S(2)}, u32[]{:S(2)}) async-start(f32[16,1,4384]{2,1,0:T(1,128)} %broadcast_in_dim.41), calls=%async_computation.2 | async-start | bytes 573440 | tf_op jit(solution)/shard_map/all_to_all | solution.py:39
  153.5 9.4 %copy-start.2 = (bf16[288,2048]{1,0:T(8,128)(2,1)S(1)}, bf16[288,2048]{1,0:T(8,128)(2,1)}, u32[]{:S(2)}) copy-start(bf16[288,2048]{1,0:T(8,128)(2,1)} %reshape.149) | copy-start | bytes 3538948
  153.5 9.4 %copy-start.16 = (bf16[288,96]{0,1:T(8,128)(2,1)S(1)}, bf16[288,96]{0,1:T(8,128)(2,1)}, u32[]{:S(2)}) copy-start(bf16[288,96]{0,1:T(8,128)(2,1)} %get-tuple-element.55) | copy-start | bytes 165892
  153.5 48.5 %all-to-all-start.1 = ((bf16[16,2,26624]{2,1,0:T(2,128)(2,1)}), bf16[16,2,26624]{2,1,0:T(2,128)(2,1)S(1)}, u32[]{:S(2)}, u32[]{:S(2)}) async-start(bf16[16,2,26624]{2,1,0:T(2,128)(2,1)} %reshape.216), calls=%async_computation.1 | async-start | bytes 3407872 | tf_op jit(solution)/shard_map/all_to_all | solution.py:24
  162.2 48.0 %copy-start.17 = (f32[2,2048]{1,0:T(2,128)}, f32[2,2048]{1,0:T(2,128)S(1)}, u32[]{:S(2)}) copy-start(f32[2,2048]{1,0:T(2,128)S(1)} %reduce_sum.110) | copy-start | bytes 49156
  221.8 27.2 %all-to-all-start.3 = ((f32[48,1,774]{2,1,0:T(1,128)}), f32[48,1,774]{2,1,0:T(1,128)S(1)}, u32[]{:S(2)}, u32[]{:S(2)}) async-start(f32[48,1,774]{2,1,0:T(1,128)} %reshape.218), calls=%async_computation.3 | async-start | bytes 344064 | tf_op jit(solution)/shard_map/all_to_all | solution.py:61
  250.9 3.2 %copy-start.12 = (f32[128,2]{1,0:T(8,128)S(1)}, f32[128,2]{1,0:T(8,128)}, u32[]{:S(2)}) copy-start(f32[128,2]{1,0:T(8,128)} %copy-done.11) | copy-start | bytes 3076
Sparse Core Ops, SparseCore 0:
  61.6 45.6 all-gather.1
where the time goes:
time: 263 us; the launch traced here: 262 us
  waiting for transfers between devices  85.5 us (33%)
  local copies, waits for them, and re-layouts  63.4 us (24%)
  blocking collectives  32.7 us (12%)
  starting transfers between devices  31.7 us (12%)
  other arithmetic  24.2 us (9%)
  between operations  14.6 us (6%)
  matrix products  10.1 us (4%)
    all_gather x1, waiting for transfers between devices, side_by_side_2(): whole, at, done = (lax.all_gather(both, axis, axis=dim, tiled=True), 0, [])  36.4 us
    all_to_all x1, waiting for transfers between devices, side_by_side(): lax.all_to_all(both, axis, split_axis=split_dim, concat_axis=concat_dim,...  36.3 us
    all_to_all x1, blocking collectives, side_by_side(): lax.all_to_all(both, axis, split_axis=split_dim, concat_axis=concat_dim,...  32.7 us
    unnamed x46, local copies, waits for them, and re-layouts  16.6 us
    unnamed x2, other arithmetic  14.1 us
    all_to_all x1, starting transfers between devices, in_one_piece(): lax.all_to_all(both, axis, split_axis=split_dim, concat_axis=concat_dim,...  13 us
    all_to_all x1, waiting for transfers between devices, in_one_piece(): lax.all_to_all(both, axis, split_axis=split_dim, concat_axis=concat_dim,...  12.7 us
    all_to_all x2, local copies, waits for them, and re-layouts, side_by_side(): lax.all_to_all(both, axis, split_axis=split_dim, concat_axis=concat_dim,...  9.46 us
  transfers between devices with their start and end apart: 5, of which 3 were waited for; matrix products, arithmetic and copies ran while one was open for 19% of the time, Pallas kernels for 0%

commit v1 on v0

v1 whole, which is shorter than its diff:
```python
import functools

import jax
import jax.numpy as jnp
from jax import lax
from jax.experimental import pallas as pl
from jax.experimental.pallas import tpu as pltpu
from jax.sharding import Mesh, PartitionSpec as P

BF = jnp.bfloat16
F32 = jnp.float32
LANES = 128


def up(n, k):
    return -(-n // k) * k


def nn(a, b):
    return lax.dot_general(a, b, (((1,), (0,)), ((), ())), preferred_element_type=F32)


def nt(a, b):
    return lax.dot_general(a, b, (((1,), (1,)), ((), ())), preferred_element_type=F32)


def tn(a, b):
    return lax.dot_general(a, b, (((0,), (0,)), ((), ())), preferred_element_type=F32)


def rows_of(shape):
    return lax.broadcasted_iota(jnp.int32, shape, 0)


def cols_of(shape):
    return lax.broadcasted_iota(jnp.int32, shape, 1)


def divided(n, by):
    return ((n.astype(F32) + 0.5) * (1.0 / by)).astype(jnp.int32)


def picked(mask):
    return mask.astype(F32).astype(BF)


def dispatch_kernel(experts, cap, share_ref, routes_ref, gates_ref, tok0, tok1, cot0, cot1, send_ref, rank_ref):
    toks = routes_ref.shape[1]
    block = 4 * cap
    route = [routes_ref[k : k + 1, :] for k in range(2)]
    ids = rows_of((experts, toks))
    named = [ids == r for r in route]
    both = picked(named[0] | named[1])
    before = picked(rows_of((toks, toks)) < cols_of((toks, toks)))
    earlier = nn(both, before)
    ranks = [jnp.sum(jnp.where(m, earlier, 0.0), axis=0, keepdims=True).astype(jnp.int32) for m in named]
    rank_ref[...] = jnp.concatenate(ranks, axis=0)
    slot = rows_of((experts * block, toks))
    first = [r * block + k for r, k in zip(route, ranks)]
    rows_x = jnp.zeros((experts * block, LANES), F32)
    rows_c = rows_x
    gate = jnp.zeros((experts * block, toks), F32)
    for n, (tok, cot) in enumerate(((tok0, cot0), (tok1, cot1))):
        at = [slot == f + 2 * n * cap for f in first]
        rows_x = rows_x + nn(picked(at[0] | at[1]), tok[...])
        at = [slot == f + (2 * n + 1) * cap for f in first]
        rows_c = rows_c + nn(picked(at[0] | at[1]), cot[...])
        for k in range(2):
            gate = jnp.where(at[k], gates_ref[k : k + 1, :], gate)
    gate = jnp.sum(gate, axis=1, keepdims=True)
    send_ref[...] = (rows_x + gate * rows_c).astype(BF)


def compact_kernel(cap, recv_ref, out_ref):
    experts = recv_ref.shape[0] // (4 * cap)
    slots = experts * cap
    group = 8 if experts % 8 == 0 else experts
    size, count = 4 * cap * group, cap * group
    row, at = rows_of((size, size)), cols_of((size, size))
    kind = divided(row, count)
    row = row - kind * count
    source = divided(row, cap)
    order = picked(at == source * (3 * cap) + row + kind * cap)
    for g in range(experts // group):
        rows = nn(order, recv_ref[g * size : (g + 1) * size, :]).astype(BF)
        for n in range(4):
            out_ref[n * slots + g * count : n * slots + (g + 1) * count, :] = rows[n * count : (n + 1) * count, :]


def swiglu_back(x, c, gate_weight, up_weight, down_weight):
    pre_gate = nt(gate_weight, x)
    pre_up = nt(up_weight, x)
    hidden_grad = nt(down_weight, c)
    s = jax.nn.sigmoid(pre_gate)
    activated = pre_gate * s
    hidden = (activated * pre_up).astype(BF)
    d_gate = (hidden_grad * pre_up * s * (1.0 + pre_gate * (1.0 - s))).astype(BF)
    d_up = (hidden_grad * activated).astype(BF)
    return hidden, hidden_grad, d_gate, d_up


def shared_kernel(tok_ref, cot_ref, gate_ref, up_ref, down_ref, piece_ref, term_ref, lined_ref):
    tok, cot = tok_ref[...], cot_ref[...]
    gate_weight, up_weight = gate_ref[...], up_ref[...]
    hidden, _, d_gate, d_up = swiglu_back(tok, cot, gate_weight, up_weight, down_ref[...])
    back = tn(
        jnp.concatenate([d_gate, d_up], axis=0), jnp.concatenate([gate_weight, up_weight], axis=0)
    ).astype(BF)
    term = nn(hidden, cot)
    for p in range(piece_ref.shape[0]):
        piece_ref[p] = back[:, p * LANES : (p + 1) * LANES]
        lined_ref[:, p, :] = term[:, p * LANES : (p + 1) * LANES]
    term_ref[...] = lined_ref[...].reshape(term_ref.shape).astype(BF)


OFFSETS = (0, 4, 7, 3, 1, 5, 6, 2)


def assemble(at_ref, own_ref, other_ref, x_ref, c_ref):
    slots = c_ref.shape[0]
    y, core = at_ref[0], at_ref[1]
    for n, offset in enumerate(OFFSETS):
        chip = lax.rem(y + offset, len(OFFSETS))
        for ref, side in ((own_ref, core), (other_ref, 1 - core)):
            lane = pl.multiple_of((2 * chip + side) * LANES, LANES)
            if x_ref is not None:
                x_ref[:, pl.ds(lane, LANES)] = ref[n, 0:slots, :]
            c_ref[:, pl.ds(lane, LANES)] = ref[n, slots : 2 * slots, :]


def expert_kernel(
    extra, at_ref, own_ref, other_ref, gate_ref, up_ref, down_ref, piece_ref,
    keep_ref, send_ref, hidden_ref, g_gate_ref, g_up_ref, x_ref, c_ref, blocks_ref,
):
    assemble(at_ref, own_ref, other_ref, x_ref, c_ref)
    slots = x_ref.shape[0]
    shares, toks, _ = piece_ref.shape
    gate_weight, up_weight = gate_ref[...], up_ref[...]
    hidden, hidden_grad, d_gate, d_up = swiglu_back(
        x_ref[...], c_ref[...], gate_weight, up_weight, down_ref[...]
    )
    hidden_ref[...] = hidden
    dots = jnp.sum(hidden.astype(F32) * hidden_grad, axis=0, keepdims=True)
    back = tn(
        jnp.concatenate([d_gate, d_up], axis=0), jnp.concatenate([gate_weight, up_weight], axis=0)
    ).astype(BF)
    for p in range(shares):
        blocks_ref[p] = back[:, p * LANES : (p + 1) * LANES]
    line = rows_of((extra, LANES))
    rest = jnp.zeros((extra, LANES), F32)
    for k, (d, out_ref) in enumerate(((d_gate, g_gate_ref), (d_up, g_up_ref))):
        g = nn(d, x_ref[...])
        out_ref[...] = g
        sums = jnp.sum(g * g, axis=0, keepdims=True)
        for p in range(shares):
            rest = jnp.where(line == k * shares + p, sums[:, p * LANES : (p + 1) * LANES], rest)
    wide = up(slots, LANES)
    dots = jnp.concatenate([dots, jnp.zeros((1, wide - slots), F32)], axis=1)
    for k in range(wide // LANES):
        rest = jnp.where(line == 2 * shares + k, dots[:, k * LANES : (k + 1) * LANES], rest)
    rest = rest.astype(BF)
    core = at_ref[1]
    for y in range(keep_ref.shape[0]):
        for ref, side in ((keep_ref, core), (send_ref, 1 - core)):
            ref[y, 0:slots, :] = blocks_ref[2 * y + side]
            ref[y, slots : slots + toks, :] = piece_ref[2 * y + side]
            ref[y, slots + toks : slots + toks + extra, :] = rest


def down_kernel(at_ref, own_ref, other_ref, hidden_ref, g_down_ref, n_down_ref, c_ref):
    assemble(at_ref, own_ref, other_ref, None, c_ref)
    g_down = nn(hidden_ref[...], c_ref[...])
    g_down_ref[...] = g_down
    n_down_ref[...] = jnp.sum(g_down * g_down, axis=1, keepdims=True) * (1.0 / g_down.shape[1])


def return_kernel(cap, block, width, parts_ref, back_ref, shared_ref, norm_ref):
    size = back_ref.shape[0]
    slots = size // block * cap
    toks = shared_ref.shape[0]
    shares = norm_ref.shape[1] // LANES
    total = parts_ref[0].astype(F32)
    for y in range(1, parts_ref.shape[0]):
        total = total + parts_ref[y].astype(F32)
    shared_ref[...] = total[slots : slots + toks, :]
    for k in range(2):
        for p in range(shares):
            at = slots + toks + k * shares + p
            norm_ref[k : k + 1, p * LANES : (p + 1) * LANES] = total[at : at + 1, :] * (1.0 / width)
    row = rows_of((size, slots))
    slot = cols_of((size, slots))
    source = divided(row, block)
    inner = row - source * block
    mask = (slot == source * cap + inner) & (inner < cap)
    back = nn(picked(mask), total[0:slots, :].astype(BF))
    row = rows_of((size, LANES))
    source = divided(row, block)
    is_dot = row == source * block + cap
    for k in range(up(slots, LANES) // LANES):
        at = slots + toks + 2 * shares + k
        dots = total[at : at + 1, :].astype(BF).astype(F32)
        mine = divided(cols_of((size, LANES)) + k * LANES, cap) == source
        left = jnp.where(is_dot & mine, dots, 0.0).astype(BF)
        number = rows_of((LANES, LANES)) + k * LANES
        place = number - divided(number, cap) * cap
        back = back + nn(left, picked(place == cols_of((LANES, LANES))))
    back_ref[...] = back.astype(BF)


def combine_kernel(cap, block, recv_ref, routes_ref, rank_ref, gates_ref, shared_ref, grad_ref, gate_grad_ref):
    size = recv_ref.shape[0]
    toks = routes_ref.shape[1]
    recv = recv_ref[...]
    row = rows_of((size, toks))
    lane = rows_of((LANES, toks))
    at = []
    for k in range(2):
        route, rank = routes_ref[k : k + 1, :], rank_ref[k : k + 1, :]
        at.append(row == route * block + rank)
        dots = tn(recv, picked(row == route * block + cap))
        dot = jnp.sum(jnp.where(lane == rank, dots, 0.0), axis=0, keepdims=True)
        gate_grad_ref[k : k + 1, :] = dot / gates_ref[k : k + 1, :]
    grad_ref[...] = (tn(picked(at[0] | at[1]), recv) + shared_ref[...]).astype(BF)


def local(body, args, outs, scratch=(), scalars=0, flops=0):
    specs = [pl.BlockSpec(memory_space=pltpu.SMEM)] * scalars
    specs = specs + [pl.BlockSpec(memory_space=pltpu.VMEM)] * (len(args) - scalars)
    return pl.pallas_call(
        body,
        in_specs=specs,
        out_shape=tuple(jax.ShapeDtypeStruct(s, d) for s, d in outs),
        out_specs=tuple(pl.BlockSpec(memory_space=pltpu.VMEM) for _ in outs),
        scratch_shapes=list(scratch),
        cost_estimate=pl.CostEstimate(flops=flops, bytes_accessed=flops // 1000, transcendentals=0),
        compiler_params=pltpu.CompilerParams(vmem_limit_bytes=40 * 1024 * 1024),
    )(*args)


def shifted(x, by, count):
    return lax.ppermute(x, "y", [(i, (i + by) % count) for i in range(count)])


def all_steps(tokens, routes, route_gates, cotangent, w_gate, w_up, w_down, s_gate, s_up, s_down):
    tp = ("y", "core")
    ep_count = lax.axis_size("ep")
    shares = lax.axis_size(tp)
    chips = shares // 2
    y = lax.axis_index("y").astype(jnp.int32)
    core = lax.axis_index("core").astype(jnp.int32)
    at = jnp.stack([y, core])
    share = jnp.stack([2 * y + core, 2 * ((y + chips // 2) % chips) + core])
    toks, width = tokens.shape
    units = w_gate.shape[2]
    cap = max(2, (9 * toks * 2 + 8 * ep_count - 1) // (8 * ep_count))
    slots = ep_count * cap
    back_block = up(cap + 1, 8)
    routes_t, gates_t = routes.T, route_gates.T

    narrow = [pl.BlockSpec((toks, LANES), lambda i, s, n=n: (0, s[n])) for n in range(2)]
    whole = pl.BlockSpec((2, toks), lambda i, s: (0, 0))
    send, ranks = pl.pallas_call(
        functools.partial(dispatch_kernel, ep_count, cap),
        out_shape=(
            jax.ShapeDtypeStruct((4 * slots, LANES), BF),
            jax.ShapeDtypeStruct((2, toks), jnp.int32),
        ),
        grid_spec=pltpu.PrefetchScalarGridSpec(
            num_scalar_prefetch=1,
            grid=(1,),
            in_specs=[whole, whole] + narrow + narrow,
            out_specs=(
                pl.BlockSpec((4 * slots, LANES), lambda i, s: (0, 0)),
                pl.BlockSpec((2, toks), lambda i, s: (0, 0)),
            ),
        ),
    )(share, routes_t, gates_t, tokens, tokens, cotangent, cotangent)
    recv = lax.all_to_all(send.reshape(ep_count, 4 * cap, LANES), "ep", 0, 0, tiled=True)

    piece, term = local(
        shared_kernel,
        (tokens, cotangent, s_gate.T, s_up.T, s_down),
        [((shares, toks, LANES), BF), ((ep_count, units * shares // ep_count, LANES), BF)],
        [pltpu.VMEM((units, shares, LANES), F32)],
        flops=4 * 10**9,
    )
    recv, piece, term = lax.optimization_barrier((recv, piece, term))
    term_parts = lax.all_to_all(term, "ep", 0, 0, tiled=True)

    (mine,) = local(
        functools.partial(compact_kernel, cap), (recv.reshape(4 * slots, LANES),), [((4 * slots, LANES), BF)]
    )
    mine = mine.reshape(2, 2 * slots, LANES)
    near = [shifted(mine, 1, chips), shifted(mine, -1, chips)]
    near.append(shifted(mine[:1], 2, chips))
    near.append(shifted(mine[:1], -2, chips))
    own = jnp.concatenate([mine] + near, axis=0)
    swap = [(0, 1), (1, 0)]
    other = lax.ppermute(own, "core", swap)

    extra = up(2 * shares + up(slots, LANES) // LANES, 16)
    wide = pltpu.VMEM((slots, width), BF)
    moved = ((chips, slots + toks + extra, LANES), BF)
    grads = ((units, width), F32)
    keep, give, hidden, g_gate, g_up = local(
        functools.partial(expert_kernel, extra),
        (at, own, other, w_gate[0].T, w_up[0].T, w_down[0], piece),
        [moved, moved, ((units, slots), BF), grads, grads],
        [wide, wide, pltpu.VMEM((shares, slots, LANES), BF)],
        scalars=1,
        flops=8 * 10**9,
    )
    taken = lax.ppermute(give, "core", swap)
    pair = (keep.astype(F32) + taken.astype(F32)).astype(BF)
    pair_parts = lax.all_to_all(pair, "y", 0, 0, tiled=True)
    g_down, n_down = local(
        down_kernel, (at, own, other, hidden), [grads, ((units, 1), F32)], [wide], scalars=1, flops=3 * 10**9
    )

    back, shared_back, norm_in = local(
        functools.partial(return_kernel, cap, back_block, units * shares),
        (pair_parts,),
        [((ep_count * back_block, LANES), BF), ((toks, LANES), F32), ((2, width), F32)],
    )
    came = lax.all_to_all(back.reshape(ep_count, back_block, LANES), "ep", 0, 0, tiled=True)
    token_grad, gate_grad = local(
        functools.partial(combine_kernel, cap, back_block),
        (came.reshape(ep_count * back_block, LANES), routes_t, ranks, gates_t, shared_back),
        [((toks, LANES), BF), ((2, toks), F32)],
    )

    grad_shared = jnp.sum(term_parts.astype(F32), axis=0).reshape(-1, width)
    norm_shared = jnp.mean(grad_shared**2, axis=1)
    return (
        token_grad,
        gate_grad.T,
        g_gate.T[None],
        g_up.T[None],
        g_down[None],
        grad_shared,
        norm_in[None],
        n_down.reshape(1, units),
        norm_shared,
    )


def solution(mesh):
    tp = ("y", "core")
    ep_count, tp_count = mesh.devices.shape
    fine = Mesh(mesh.devices.reshape(ep_count, tp_count // 2, 2), ("ep", "y", "core"))
    placed = (
        P("ep", None),
        P("ep", None),
        P("ep", None),
        P("ep", None),
        P("ep", None, tp),
        P("ep", None, tp),
        P("ep", tp, None),
        P(None, tp),
        P(None, tp),
        P(tp, None),
    )
    return jax.shard_map(
        all_steps,
        mesh=fine,
        in_specs=placed,
        out_specs=(
            P("ep", tp),
            P("ep", None),
            P("ep", None, tp),
            P("ep", None, tp),
            P("ep", tp, None),
            P(("y", "core", "ep"), None),
            P("ep", None, None),
            P("ep", tp),
            P(("y", "core", "ep")),
        ),
        check_vma=False,
    )
```

time: 263 us -> 154 us (0.59)
  local copies, waits for them, and re-layouts: 63.4 us -> 1.7 us
  blocking collectives: 32.7 us -> 0 us
  starting transfers between devices: 31.7 us -> 58.6 us
  other arithmetic: 24.2 us -> 5.55 us
  Pallas kernels: 0 us -> 15.2 us
  waiting for transfers between devices: 85.5 us -> 71.7 us
  between operations: 14.6 us -> 0.92 us
  matrix products: 10.1 us -> 0 us
    all_gather x1 -> x0, waiting for transfers between devices: 36.4 us -> none  [side_by_side_2(): whole, at, done = (lax.all_gather(both, axis, axis=dim, tiled=True), 0, [])]
    all_to_all x1 -> x0, blocking collectives: 32.7 us -> none  [side_by_side(): lax.all_to_all(both, axis, split_axis=split_dim, concat_axis=concat_dim,...]
    ppermute x0 -> x6, starting transfers between devices: none -> 22.3 us  [the longest x4 13.3 us: shifted(): return lax.ppermute(x, 'y', [(i, (i + by) % count) for i in range(count)])]
    unnamed x46 -> x30, local copies, waits for them, and re-layouts: 16.6 us -> 0.97 us
    pallas_call x0 -> x7, Pallas kernels: none -> 15.2 us  [the longest x6 11.8 us: local(): pl.pallas_call(body, in_specs=specs, out_shape=tuple((jax.ShapeDtypeStruc...]
    unnamed x2 -> x0, other arithmetic: 14.1 us -> none
    all_to_all x4, waiting for transfers between devices: 49.1 us -> 62.9 us  [the longest x1 23.4 us: all_steps(): pair_parts = lax.all_to_all(pair, 'y', 0, 0, tiled=True)]
    dot_general x12 -> x0, matrix products: 10.1 us -> none  [the longest x2 2.61 us: swiglu_back(): pre_gate = jnp.dot(rows_x, gate_weight, preferred_element_type=jnp.float32)]
  transfers between devices with their start and end apart: 5 -> 10, of which waited for: 3 -> 7; matrix products, arithmetic and copies ran while one was open for 19% -> 4% of each run, Pallas kernels for 0% -> 3%
where the time goes in v1:
time: 154 us
  waiting for transfers between devices  71.7 us (47%)
  starting transfers between devices  58.6 us (38%)
  Pallas kernels  15.2 us (10%)
  other arithmetic  5.55 us (4%)
  local copies, waits for them, and re-layouts  1.7 us (1%)
    all_to_all x1, waiting for transfers between devices, all_steps(): pair_parts = lax.all_to_all(pair, 'y', 0, 0, tiled=True)  23.4 us
    all_to_all x1, starting transfers between devices, all_steps(): lax.all_to_all(send.reshape(ep_count, 4 * cap, LANES), 'ep', 0, 0, tiled=...  18.8 us
    all_to_all x1, waiting for transfers between devices, all_steps(): term_parts = lax.all_to_all(term, 'ep', 0, 0, tiled=True)  17.6 us
    all_to_all x1, waiting for transfers between devices, all_steps(): lax.all_to_all(send.reshape(ep_count, 4 * cap, LANES), 'ep', 0, 0, tiled=...  14.5 us
    ppermute x4, starting transfers between devices, shifted(): return lax.ppermute(x, 'y', [(i, (i + by) % count) for i in range(count)])  13.3 us
    pallas_call x6, Pallas kernels, local(): pl.pallas_call(body, in_specs=specs, out_shape=tuple((jax.ShapeDtypeStruc...  11.8 us
    all_to_all x1, starting transfers between devices, all_steps(): lax.all_to_all(back.reshape(ep_count, back_block, LANES), 'ep', 0, 0, til...  8.64 us
    all_to_all x1, waiting for transfers between devices, all_steps(): lax.all_to_all(back.reshape(ep_count, back_block, LANES), 'ep', 0, 0, til...  7.44 us
  transfers between devices with their start and end apart: 10, of which 7 were waited for; matrix products, arithmetic and copies ran while one was open for 4% of the time, Pallas kernels for 3%

profile of v1, /device:TPU:1, one launch (start us, length us, event | category | flops | bytes accessed | tf_op | source)
XLA Modules:
  0.0 153.7 jit_solution(7082952604602366713)
XLA Ops:
  0.7 0.6 pad_add_fusion.1.share_ref
  1.3 0.0 copy-start.7
  1.3 3.4 %shard_map.169 = (bf16[1152,128]{1,0:T(8,128)(2,1)}, s32[2,128]{1,0:T(2,128)}) custom-call(s32[2]{0:T(128)} %pad_add_fusion.1.share_ref, s32[2,128]{1,0:T(2,128)} %bitcast.37, f32[2,128]{1,0:T(2,128)} %bitcast.39, bf16[128,2048]{1,0:T(8,128)(2,1)} %tok_ref.1, bf16[128,2048]{1,0:T(8,128)(2,1)} %tok_ref.1, bf16[128,2048]{1,0:T(8,128)(2,1)} %cot_ref.1, ...), custom_call_target="tpu_custom_call" | custom-call | tf_op jit(solution)/shard_map/pallas_call | solution.py:262
  4.6 18.8 %all-to-all-start = ((bf16[48,24,128]{2,1,0:T(8,128)(2,1)}), bf16[48,24,128]{2,1,0:T(8,128)(2,1)S(1)}, u32[]{:S(2)}, u32[]{:S(2)}) async-start(bf16[48,24,128]{2,1,0:T(8,128)(2,1)} %bitcast.46), calls=%async_computation | async-start | bytes 589824 | tf_op jit(solution)/shard_map/all_to_all | solution.py:278
  23.5 0.0 copy-done
  23.5 0.0 copy-done.1
  23.5 0.0 copy-done.5
  23.5 2.3 %shard_map.170 = (bf16[16,128,128]{2,1,0:T(8,128)(2,1)S(1)}, bf16[48,32,128]{2,1,0:T(8,128)(2,1)}) custom-call(bf16[128,2048]{1,0:T(8,128)(2,1)S(1)} %copy-done, bf16[128,2048]{1,0:T(8,128)(2,1)S(1)} %copy-done.1, bf16[96,2048]{1,0:T(8,128)(2,1)S(1)} %bitcast.41, bf16[96,2048]{1,0:T(8,128)(2,1)S(1)} %bitcast.42, bf16[96,2048]{1,0:T(8,128)(2,1)S(1)} %copy-done.7), custom_call_target="tpu_custom_call" | custom-call | flops 4000000000 | bytes 4000000 | tf_op jit(solution)/shard_map/pallas_call | solution.py:229
  25.8 0.8 copy-done.11
  26.6 14.5 %all-to-all-done = bf16[48,24,128]{2,1,0:T(8,128)(2,1)S(1)} async-done(((bf16[48,24,128]{2,1,0:T(8,128)(2,1)}), bf16[48,24,128]{2,1,0:T(8,128)(2,1)S(1)}, u32[]{:S(2)}, u32[]{:S(2)}) %all-to-all-start) | async-done | bytes 294944 | tf_op jit(solution)/shard_map/all_to_all | solution.py:278
  41.1 0.3 shard_map.171
  41.4 5.1 %collective-permute-start.1 = (bf16[2,576,128]{2,1,0:T(8,128)(2,1)S(1)}, bf16[2,576,128]{2,1,0:T(8,128)(2,1)S(1)}, u32[]{:S(2)}, u32[]{:S(2)}) collective-permute-start(bf16[2,576,128]{2,1,0:T(8,128)(2,1)S(1)} %bitcast.32), channel_id=1, source_target_pairs={{0,14},{2,0},{4,2},{6,4},{8,6},{10,8},{12,10},{14,12},{1,15},{3,1}... | collective-permute-start | bytes 884744 | tf_op jit(solution)/shard_map/ppermute | solution.py:241
  46.5 1.9 %collective-permute-start = (bf16[2,576,128]{2,1,0:T(8,128)(2,1)S(1)}, bf16[2,576,128]{2,1,0:T(8,128)(2,1)S(1)}, u32[]{:S(2)}, u32[]{:S(2)}) collective-permute-start(bf16[2,576,128]{2,1,0:T(8,128)(2,1)S(1)} %bitcast.33), channel_id=1, source_target_pairs={{0,2},{2,4},{4,6},{6,8},{8,10},{10,12},{12,14},{14,0},{1,3},{3,5},... | collective-permute-start | bytes 884744 | tf_op jit(solution)/shard_map/ppermute | solution.py:241
  48.4 0.0 copy-start.8
  48.4 0.0 copy-start.9
  48.5 0.0 copy-start.10
  48.5 0.0 copy-start.12
  48.5 4.3 %collective-permute-start.3 = (bf16[1,576,128]{2,1,0:T(8,128)(2,1)S(1)}, bf16[1,576,128]{2,1,0:T(8,128)(2,1)S(1)}, u32[]{:S(2)}, u32[]{:S(2)}) collective-permute-start(bf16[1,576,128]{2,1,0:T(8,128)(2,1)S(1)} %slice_bitcast_fusion), channel_id=1, source_target_pairs={{0,12},{2,14},{4,0},{6,2},{8,4},{10,6},{12,8},{14,10},{1,13},{3,15... | collective-permute-start | bytes 442376 | tf_op jit(solution)/shard_map/ppermute | solution.py:241
  52.8 2.0 %collective-permute-start.2 = (bf16[1,576,128]{2,1,0:T(8,128)(2,1)S(1)}, bf16[1,576,128]{2,1,0:T(8,128)(2,1)S(1)}, u32[]{:S(2)}, u32[]{:S(2)}) collective-permute-start(bf16[1,576,128]{2,1,0:T(8,128)(2,1)S(1)} %slice_bitcast_fusion), channel_id=1, source_target_pairs={{0,4},{2,6},{4,8},{6,10},{8,12},{10,14},{12,0},{14,2},{1,5},{3,7},... | collective-permute-start | bytes 442376 | tf_op jit(solution)/shard_map/ppermute | solution.py:241
  54.8 1.0 collective-permute-done
  55.8 0.0 collective-permute-done.1
  55.9 5.4 %collective-permute-done.2 = bf16[1,576,128]{2,1,0:T(8,128)(2,1)S(1)} collective-permute-done((bf16[1,576,128]{2,1,0:T(8,128)(2,1)S(1)}, bf16[1,576,128]{2,1,0:T(8,128)(2,1)S(1)}, u32[]{:S(2)}, u32[]{:S(2)}) %collective-permute-start.2) | collective-permute-done | bytes 147488 | tf_op jit(solution)/shard_map/ppermute | solution.py:241
  61.4 0.0 collective-permute-done.3
  61.4 6.7 %collective-permute-start.4 = (bf16[8,576,128]{2,1,0:T(8,128)(2,1)S(1)}, bf16[8,576,128]{2,1,0:T(8,128)(2,1)S(1)}, u32[]{:S(2)}, u32[]{:S(2)}) collective-permute-start(bf16[8,576,128]{2,1,0:T(8,128)(2,1)S(1)} %constant_dynamic-update-slice_fusion.own_ref), channel_id=1, source_target_pairs={{0,1},{1,0},{2,3},{3,2},{4,5},{5,4},{6,7},{7,6},{8,9},{9,8},{10,11... | collective-permute-start | bytes 3538952 | tf_op jit(solution)/shard_map/ppermute | solution.py:299
  68.1 0.1 pad_add_fusion.at_ref
  68.1 2.4 %collective-permute-done.4.other_ref = bf16[8,576,128]{2,1,0:T(8,128)(2,1)S(1)} collective-permute-done((bf16[8,576,128]{2,1,0:T(8,128)(2,1)S(1)}, bf16[8,576,128]{2,1,0:T(8,128)(2,1)S(1)}, u32[]{:S(2)}, u32[]{:S(2)}) %collective-permute-start.4) | collective-permute-done | bytes 1179680 | tf_op jit(solution)/shard_map/ppermute | solution.py:299
  70.5 0.0 copy-done.10
  70.5 5.0 %shard_map.172 = (bf16[8,464,128]{2,1,0:T(8,128)(2,1)S(1)}, bf16[8,464,128]{2,1,0:T(8,128)(2,1)}, bf16[96,288]{1,0:T(8,128)(2,1)S(1)}, f32[96,2048]{1,0:T(8,128)}, f32[96,2048]{1,0:T(8,128)}) custom-call(s32[2]{0:T(128)S(1)} %pad_add_fusion.at_ref, bf16[8,576,128]{2,1,0:T(8,128)(2,1)S(1)} %constant_dynamic-update-slice_fusion.own_ref, ...), custom_call_target="tpu_custom_call" | custom-call | flops 8000000000 | bytes 8000000 | tf_op jit(solution)/shard_map/pallas_call | solution.py:229
  75.6 2.3 %collective-permute-start.5 = (bf16[8,464,128]{2,1,0:T(8,128)(2,1)}, bf16[8,464,128]{2,1,0:T(8,128)(2,1)}, u32[]{:S(2)}, u32[]{:S(2)}) collective-permute-start(bf16[8,464,128]{2,1,0:T(8,128)(2,1)} %get-tuple-element.34), channel_id=1, source_target_pairs={{0,1},{1,0},{2,3},{3,2},{4,5},{5,4},{6,7},{7,6},{8,9},{9,8},{10,11... | collective-permute-start | bytes 2850824 | tf_op jit(solution)/shard_map/ppermute | solution.py:313
  77.8 5.3 %all-to-all-start.3 = ((bf16[48,32,128]{2,1,0:T(8,128)(2,1)}), bf16[48,32,128]{2,1,0:T(8,128)(2,1)}, u32[]{:S(2)}, u32[]{:S(2)}) async-start(bf16[48,32,128]{2,1,0:T(8,128)(2,1)} %get-tuple-element.44), calls=%async_computation.3 | async-start | bytes 786432 | tf_op jit(solution)/shard_map/all_to_all | solution.py:288
  83.2 0.0 collective-permute-done.5
  83.2 2.4 %add_convert_fusion = bf16[8,464,128]{2,1,0:T(8,128)(2,1)} fusion(bf16[8,464,128]{2,1,0:T(8,128)(2,1)} %collective-permute-done.5, bf16[8,464,128]{2,1,0:T(8,128)(2,1)S(1)} %get-tuple-element.33), kind=kLoop, calls=%fused_computation | loop fusion | flops 1900544 | bytes 2850816 | tf_op jit(solution)/shard_map/convert_element_type | solution.py:314
  85.6 17.6 %all-to-all-done.3 = bf16[48,32,128]{2,1,0:T(8,128)(2,1)} async-done(((bf16[48,32,128]{2,1,0:T(8,128)(2,1)}), bf16[48,32,128]{2,1,0:T(8,128)(2,1)}, u32[]{:S(2)}, u32[]{:S(2)}) %all-to-all-start.3) | async-done | bytes 393248 | tf_op jit(solution)/shard_map/all_to_all | solution.py:288
  103.2 3.6 %all-to-all-start.1 = ((bf16[8,464,128]{2,1,0:T(8,128)(2,1)}), bf16[8,464,128]{2,1,0:T(8,128)(2,1)S(1)}, u32[]{:S(2)}, u32[]{:S(2)}) async-start(bf16[8,464,128]{2,1,0:T(8,128)(2,1)} %add_convert_fusion), calls=%async_computation.1 | async-start | bytes 1900544 | tf_op jit(solution)/shard_map/all_to_all | solution.py:315
  106.8 1.1 convert_reduce_fusion
  107.9 0.1 multiply_reduce_fusion
  108.0 0.1 reduce_sum.27
  108.1 0.1 reduce_sum.28
  108.2 23.4 %all-to-all-done.1.parts_ref = bf16[8,464,128]{2,1,0:T(8,128)(2,1)S(1)} async-done(((bf16[8,464,128]{2,1,0:T(8,128)(2,1)}), bf16[8,464,128]{2,1,0:T(8,128)(2,1)S(1)}, u32[]{:S(2)}, u32[]{:S(2)}) %all-to-all-start.1) | async-done | bytes 950304 | tf_op jit(solution)/shard_map/all_to_all | solution.py:315
  131.6 1.2 shard_map.173
  132.8 8.6 %all-to-all-start.2 = ((bf16[48,8,128]{2,1,0:T(8,128)(2,1)}), bf16[48,8,128]{2,1,0:T(8,128)(2,1)S(1)}, u32[]{:S(2)}, u32[]{:S(2)}) async-start(bf16[48,8,128]{2,1,0:T(8,128)(2,1)} %bitcast.17), calls=%async_computation.2 | async-start | bytes 196608 | tf_op jit(solution)/shard_map/all_to_all | solution.py:325
  141.4 0.5 broadcast_multiply_fusion
  141.9 0.6 reshape.46
  142.6 2.2 %shard_map.175 = (f32[96,2048]{1,0:T(8,128)}, f32[96,1]{1,0:T(8,128)S(1)}) custom-call(s32[2]{0:T(128)S(1)} %pad_add_fusion.at_ref, bf16[8,576,128]{2,1,0:T(8,128)(2,1)S(1)} %constant_dynamic-update-slice_fusion.own_ref, bf16[8,576,128]{2,1,0:T(8,128)(2,1)S(1)} %collective-permute-done.4.other_ref, bf16[96,288]{1,0:T(8,128)(2,1)S(1)} %get-tuple-element.42.hidden_ref), custom_call_target="tpu_custom_call" | custom-call | flops 3000000000 | bytes 3000000 | tf_op jit(solution)/shard_map/pallas_call | solution.py:229
  144.7 0.6 reduce.2
  145.4 7.4 %all-to-all-done.2 = bf16[48,8,128]{2,1,0:T(8,128)(2,1)S(1)} async-done(((bf16[48,8,128]{2,1,0:T(8,128)(2,1)}), bf16[48,8,128]{2,1,0:T(8,128)(2,1)S(1)}, u32[]{:S(2)}, u32[]{:S(2)}) %all-to-all-start.2) | async-done | bytes 98336 | tf_op jit(solution)/shard_map/all_to_all | solution.py:325
  152.8 0.0 copy-done.3
  152.8 0.9 shard_map.174
  (21 shorter events, 0.2 us)
Async XLA Ops:
  1.2 22.2 %copy-start = (bf16[128,2048]{1,0:T(8,128)(2,1)S(1)}, bf16[128,2048]{1,0:T(8,128)(2,1)}, u32[]{:S(2)}) copy-start(bf16[128,2048]{1,0:T(8,128)(2,1)} %tok_ref.1) | copy-start | bytes 1572868
  1.2 22.2 %copy-start.1 = (bf16[128,2048]{1,0:T(8,128)(2,1)S(1)}, bf16[128,2048]{1,0:T(8,128)(2,1)}, u32[]{:S(2)}) copy-start(bf16[128,2048]{1,0:T(8,128)(2,1)} %cot_ref.1) | copy-start | bytes 1572868
  1.3 22.2 %copy-start.5 = (bf16[2048,96]{0,1:T(8,128)(2,1)S(1)}, bf16[2048,96]{0,1:T(8,128)(2,1)}, u32[]{:S(2)}) copy-start(bf16[2048,96]{0,1:T(8,128)(2,1)} %param.17) | copy-start | bytes 1179652
  1.3 22.2 %copy-start.6 = (bf16[2048,96]{0,1:T(8,128)(2,1)S(1)}, bf16[2048,96]{0,1:T(8,128)(2,1)}, u32[]{:S(2)}) copy-start(bf16[2048,96]{0,1:T(8,128)(2,1)} %param.18) | copy-start | bytes 1179652
  1.3 22.2 %copy-start.7 = (bf16[96,2048]{1,0:T(8,128)(2,1)S(1)}, bf16[96,2048]{1,0:T(8,128)(2,1)}, u32[]{:S(2)}) copy-start(bf16[96,2048]{1,0:T(8,128)(2,1)} %down_ref.1) | copy-start | bytes 1179652
  4.6 36.4 %all-to-all-start = ((bf16[48,24,128]{2,1,0:T(8,128)(2,1)}), bf16[48,24,128]{2,1,0:T(8,128)(2,1)S(1)}, u32[]{:S(2)}, u32[]{:S(2)}) async-start(bf16[48,24,128]{2,1,0:T(8,128)(2,1)} %bitcast.46), calls=%async_computation | async-start | bytes 589824 | tf_op jit(solution)/shard_map/all_to_all | solution.py:278
  25.8 0.8 copy-start.11
  41.4 14.5 %collective-permute-start.1 = (bf16[2,576,128]{2,1,0:T(8,128)(2,1)S(1)}, bf16[2,576,128]{2,1,0:T(8,128)(2,1)S(1)}, u32[]{:S(2)}, u32[]{:S(2)}) collective-permute-start(bf16[2,576,128]{2,1,0:T(8,128)(2,1)S(1)} %bitcast.32), channel_id=1, source_target_pairs={{0,14},{2,0},{4,2},{6,4},{8,6},{10,8},{12,10},{14,12},{1,15},{3,1}... | collective-permute-start | bytes 884744 | tf_op jit(solution)/shard_map/ppermute | solution.py:241
  46.5 9.3 %collective-permute-start = (bf16[2,576,128]{2,1,0:T(8,128)(2,1)S(1)}, bf16[2,576,128]{2,1,0:T(8,128)(2,1)S(1)}, u32[]{:S(2)}, u32[]{:S(2)}) collective-permute-start(bf16[2,576,128]{2,1,0:T(8,128)(2,1)S(1)} %bitcast.33), channel_id=1, source_target_pairs={{0,2},{2,4},{4,6},{6,8},{8,10},{10,12},{12,14},{14,0},{1,3},{3,5},... | collective-permute-start | bytes 884744 | tf_op jit(solution)/shard_map/ppermute | solution.py:241
  48.4 22.1 %copy-start.8 = (bf16[1,2048,96]{1,2,0:T(8,128)(2,1)S(1)}, bf16[1,2048,96]{1,2,0:T(8,128)(2,1)}, u32[]{:S(2)}) copy-start(bf16[1,2048,96]{1,2,0:T(8,128)(2,1)} %param.14) | copy-start | bytes 1179652
  48.4 22.1 %copy-start.9 = (bf16[1,2048,96]{1,2,0:T(8,128)(2,1)S(1)}, bf16[1,2048,96]{1,2,0:T(8,128)(2,1)}, u32[]{:S(2)}) copy-start(bf16[1,2048,96]{1,2,0:T(8,128)(2,1)} %param.15) | copy-start | bytes 1179652
  48.5 22.1 %copy-start.10 = (bf16[1,96,2048]{2,1,0:T(8,128)(2,1)S(1)}, bf16[1,96,2048]{2,1,0:T(8,128)(2,1)}, u32[]{:S(2)}) copy-start(bf16[1,96,2048]{2,1,0:T(8,128)(2,1)} %param.16) | copy-start | bytes 1179652
  48.5 22.1 %copy-start.12 = (bf16[16,128,128]{2,1,0:T(8,128)(2,1)S(1)}, bf16[16,128,128]{2,1,0:T(8,128)(2,1)}, u32[]{:S(2)}) copy-start(bf16[16,128,128]{2,1,0:T(8,128)(2,1)} %copy-done.11) | copy-start | bytes 1572868
  48.5 12.9 %collective-permute-start.3 = (bf16[1,576,128]{2,1,0:T(8,128)(2,1)S(1)}, bf16[1,576,128]{2,1,0:T(8,128)(2,1)S(1)}, u32[]{:S(2)}, u32[]{:S(2)}) collective-permute-start(bf16[1,576,128]{2,1,0:T(8,128)(2,1)S(1)} %slice_bitcast_fusion), channel_id=1, source_target_pairs={{0,12},{2,14},{4,0},{6,2},{8,4},{10,6},{12,8},{14,10},{1,13},{3,15... | collective-permute-start | bytes 442376 | tf_op jit(solution)/shard_map/ppermute | solution.py:241
  52.8 8.6 %collective-permute-start.2 = (bf16[1,576,128]{2,1,0:T(8,128)(2,1)S(1)}, bf16[1,576,128]{2,1,0:T(8,128)(2,1)S(1)}, u32[]{:S(2)}, u32[]{:S(2)}) collective-permute-start(bf16[1,576,128]{2,1,0:T(8,128)(2,1)S(1)} %slice_bitcast_fusion), channel_id=1, source_target_pairs={{0,4},{2,6},{4,8},{6,10},{8,12},{10,14},{12,0},{14,2},{1,5},{3,7},... | collective-permute-start | bytes 442376 | tf_op jit(solution)/shard_map/ppermute | solution.py:241
  61.4 9.1 %collective-permute-start.4 = (bf16[8,576,128]{2,1,0:T(8,128)(2,1)S(1)}, bf16[8,576,128]{2,1,0:T(8,128)(2,1)S(1)}, u32[]{:S(2)}, u32[]{:S(2)}) collective-permute-start(bf16[8,576,128]{2,1,0:T(8,128)(2,1)S(1)} %constant_dynamic-update-slice_fusion.own_ref), channel_id=1, source_target_pairs={{0,1},{1,0},{2,3},{3,2},{4,5},{5,4},{6,7},{7,6},{8,9},{9,8},{10,11... | collective-permute-start | bytes 3538952 | tf_op jit(solution)/shard_map/ppermute | solution.py:299
  75.6 7.6 %collective-permute-start.5 = (bf16[8,464,128]{2,1,0:T(8,128)(2,1)}, bf16[8,464,128]{2,1,0:T(8,128)(2,1)}, u32[]{:S(2)}, u32[]{:S(2)}) collective-permute-start(bf16[8,464,128]{2,1,0:T(8,128)(2,1)} %get-tuple-element.34), channel_id=1, source_target_pairs={{0,1},{1,0},{2,3},{3,2},{4,5},{5,4},{6,7},{7,6},{8,9},{9,8},{10,11... | collective-permute-start | bytes 2850824 | tf_op jit(solution)/shard_map/ppermute | solution.py:313
  77.8 25.4 %all-to-all-start.3 = ((bf16[48,32,128]{2,1,0:T(8,128)(2,1)}), bf16[48,32,128]{2,1,0:T(8,128)(2,1)}, u32[]{:S(2)}, u32[]{:S(2)}) async-start(bf16[48,32,128]{2,1,0:T(8,128)(2,1)} %get-tuple-element.44), calls=%async_computation.3 | async-start | bytes 786432 | tf_op jit(solution)/shard_map/all_to_all | solution.py:288
  103.2 28.4 %all-to-all-start.1 = ((bf16[8,464,128]{2,1,0:T(8,128)(2,1)}), bf16[8,464,128]{2,1,0:T(8,128)(2,1)S(1)}, u32[]{:S(2)}, u32[]{:S(2)}) async-start(bf16[8,464,128]{2,1,0:T(8,128)(2,1)} %add_convert_fusion), calls=%async_computation.1 | async-start | bytes 1900544 | tf_op jit(solution)/shard_map/all_to_all | solution.py:315
  132.8 20.0 %all-to-all-start.2 = ((bf16[48,8,128]{2,1,0:T(8,128)(2,1)}), bf16[48,8,128]{2,1,0:T(8,128)(2,1)S(1)}, u32[]{:S(2)}, u32[]{:S(2)}) async-start(bf16[48,8,128]{2,1,0:T(8,128)(2,1)} %bitcast.17), calls=%async_computation.2 | async-start | bytes 196608 | tf_op jit(solution)/shard_map/all_to_all | solution.py:325
  142.5 10.3 %copy-start.2 = (s32[128,2]{0,1:T(2,128)S(1)}, s32[128,2]{0,1:T(2,128)}, u32[]{:S(2)}) copy-start(s32[128,2]{0,1:T(2,128)} %param.11) | copy-start | bytes 3076
  142.5 10.3 %copy-start.3 = (f32[128,2]{0,1:T(2,128)S(1)}, f32[128,2]{0,1:T(2,128)}, u32[]{:S(2)}) copy-start(f32[128,2]{0,1:T(2,128)} %param.12) | copy-start | bytes 3076
  142.6 10.3 %copy-start.4 = (s32[2,128]{1,0:T(2,128)S(1)}, s32[2,128]{1,0:T(2,128)}, u32[]{:S(2)}) copy-start(s32[2,128]{1,0:T(2,128)} %get-tuple-element.36.rank_ref) | copy-start | bytes 3076

commit v2 on v1

v2 whole, which is shorter than its diff:
```python
import functools

import jax
import jax.numpy as jnp
from jax import lax
from jax.experimental import pallas as pl
from jax.experimental.pallas import tpu as pltpu
from jax.sharding import Mesh, PartitionSpec as P

BF = jnp.bfloat16
F32 = jnp.float32
LANES = 128


def up(n, k):
    return -(-n // k) * k


def nn(a, b):
    return lax.dot_general(a, b, (((1,), (0,)), ((), ())), preferred_element_type=F32)


def nt(a, b):
    return lax.dot_general(a, b, (((1,), (1,)), ((), ())), preferred_element_type=F32)


def tn(a, b):
    return lax.dot_general(a, b, (((0,), (0,)), ((), ())), preferred_element_type=F32)


def rows_of(shape):
    return lax.broadcasted_iota(jnp.int32, shape, 0)


def cols_of(shape):
    return lax.broadcasted_iota(jnp.int32, shape, 1)


def divided(n, by):
    return ((n.astype(F32) + 0.5) * (1.0 / by)).astype(jnp.int32)


def picked(mask):
    return mask.astype(F32).astype(BF)


def groups_of(experts):
    return 8 if experts % 8 == 0 else experts


def regroup(cap, group, to_kinds):
    size, count = 4 * cap * group, cap * group
    kinds, sources = rows_of((size, size)), cols_of((size, size))
    if not to_kinds:
        kinds, sources = sources, kinds
    kind = divided(kinds, count)
    kinds = kinds - kind * count
    source = divided(kinds, cap)
    return picked(sources == source * (3 * cap) + kinds + kind * cap)


def dispatch_kernel(experts, cap, share_ref, routes_ref, gates_ref, tok0, tok1, cot0, cot1, send_ref, rank_ref):
    toks = routes_ref.shape[1]
    slots = experts * cap
    route = [routes_ref[k : k + 1, :] for k in range(2)]
    ids = rows_of((experts, toks))
    named = [ids == r for r in route]
    both = picked(named[0] | named[1])
    before = picked(rows_of((toks, toks)) < cols_of((toks, toks)))
    earlier = nn(both, before)
    ranks = [jnp.sum(jnp.where(m, earlier, 0.0), axis=0, keepdims=True).astype(jnp.int32) for m in named]
    rank_ref[...] = jnp.concatenate(ranks, axis=0)
    slot = rows_of((slots, toks))
    same = rows_of((toks, toks)) == cols_of((toks, toks))
    toks_both = jnp.concatenate([tok0[...], tok1[...]], axis=1)
    cots_both = jnp.concatenate([cot0[...], cot1[...]], axis=1).astype(F32)
    rows_x = rows_c = None
    for k in range(2):
        at = picked(slot == route[k] * cap + ranks[k])
        gate = jnp.sum(jnp.where(same, gates_ref[k : k + 1, :], 0.0), axis=1, keepdims=True)
        x, c = nn(at, toks_both), nn(at, (gate * cots_both).astype(BF))
        rows_x, rows_c = (x, c) if rows_x is None else (rows_x + x, rows_c + c)
    rows_x, rows_c = rows_x.astype(BF), rows_c.astype(BF)
    group = groups_of(experts)
    order = regroup(cap, group, False)
    size, count = 4 * cap * group, cap * group
    for g in range(experts // group):
        rows = slice(g * count, (g + 1) * count)
        kinds = [m[rows, n * LANES : (n + 1) * LANES] for n in range(2) for m in (rows_x, rows_c)]
        send_ref[g * size : (g + 1) * size, :] = nn(order, jnp.concatenate(kinds, axis=0)).astype(BF)


def compact_kernel(cap, recv_ref, keep_ref, taken_ref, up_ref, down_ref, far_up_ref, far_down_ref, stay_ref):
    experts = recv_ref.shape[0] // (4 * cap)
    slots = experts * cap
    toks = keep_ref.shape[1]
    group = groups_of(experts)
    size, count = 4 * cap * group, cap * group
    order = regroup(cap, group, True)
    for g in range(experts // group):
        rows = nn(order, recv_ref[g * size : (g + 1) * size, :]).astype(BF)
        for n in range(4):
            at = slice(n * slots + g * count, n * slots + (g + 1) * count)
            part = rows[n * count : (n + 1) * count, :]
            up_ref[at, :] = part
            down_ref[at, :] = part
            if n < 2:
                far_up_ref[at, :] = part
                far_down_ref[at, :] = part
    near, far = 4 * slots, 2 * slots
    for n, (ref, at) in enumerate(
        ((up_ref, near), (up_ref, near + toks), (down_ref, near), (down_ref, near + toks), (far_up_ref, far), (far_down_ref, far))
    ):
        ref[at : at + toks, :] = (keep_ref[n].astype(F32) + taken_ref[n].astype(F32)).astype(BF)
    for n in range(2):
        stay_ref[n] = keep_ref[6 + n].astype(F32) + taken_ref[6 + n].astype(F32)


def join_kernel(mine_ref, up_ref, down_ref, far_up_ref, far_down_ref, stay_ref, own_ref, near_ref, far_ref):
    rows = own_ref.shape[1]
    toks = near_ref.shape[0]
    at = 0
    for ref, count in ((mine_ref, 2), (up_ref, 2), (down_ref, 2), (far_up_ref, 1), (far_down_ref, 1)):
        for n in range(count):
            own_ref[at] = ref[n * rows : (n + 1) * rows, :]
            at += 1
    near = stay_ref[0]
    for ref, count in ((up_ref, 2), (down_ref, 2), (far_up_ref, 1), (far_down_ref, 1)):
        near = near + ref[count * rows : count * rows + toks, :].astype(F32)
    near_ref[...] = near
    far = stay_ref[1]
    for ref in (up_ref, down_ref):
        far = far + ref[2 * rows + toks : 2 * rows + 2 * toks, :].astype(F32)
    far_ref[...] = far.astype(BF)


def swiglu_back(x, c, gate_weight, up_weight, down_weight):
    pre_gate = nt(gate_weight, x)
    pre_up = nt(up_weight, x)
    hidden_grad = nt(down_weight, c)
    s = jax.nn.sigmoid(pre_gate)
    activated = pre_gate * s
    hidden = (activated * pre_up).astype(BF)
    d_gate = (hidden_grad * pre_up * s * (1.0 + pre_gate * (1.0 - s))).astype(BF)
    d_up = (hidden_grad * activated).astype(BF)
    return hidden, hidden_grad, d_gate, d_up


ORDER = (1, 5, 7, 3, 2, 6, 0, 4)


def shared_kernel(
    at_ref, tok_ref, cot_ref, gate_ref, up_ref, down_ref, keep_ref, send_ref, term_ref, lined_ref, blocks_ref
):
    tok, cot = tok_ref[...], cot_ref[...]
    gate_weight, up_weight = gate_ref[...], up_ref[...]
    hidden, _, d_gate, d_up = swiglu_back(tok, cot, gate_weight, up_weight, down_ref[...])
    back = tn(
        jnp.concatenate([d_gate, d_up], axis=0), jnp.concatenate([gate_weight, up_weight], axis=0)
    ).astype(BF)
    term = nn(hidden, cot)
    for p in range(blocks_ref.shape[0]):
        blocks_ref[p] = back[:, p * LANES : (p + 1) * LANES]
        lined_ref[:, p, :] = term[:, p * LANES : (p + 1) * LANES]
    term_ref[...] = lined_ref[...].reshape(term_ref.shape).astype(BF)
    y, core = at_ref[0] >> 1, at_ref[0] & 1
    for n, offset in enumerate(ORDER):
        chip = lax.rem(y + offset, len(ORDER))
        keep_ref[n] = blocks_ref[2 * chip + core]
        send_ref[n] = blocks_ref[2 * chip + 1 - core]


OFFSETS = (0, 4, 7, 3, 1, 5, 6, 2)


def assemble(at_ref, own_ref, other_ref, x_ref, c_ref):
    slots = c_ref.shape[0]
    y, core = at_ref[0] >> 1, at_ref[0] & 1
    for n, offset in enumerate(OFFSETS):
        chip = lax.rem(y + offset, len(OFFSETS))
        for ref, side in ((own_ref, core), (other_ref, 1 - core)):
            lane = pl.multiple_of((2 * chip + side) * LANES, LANES)
            if x_ref is not None:
                x_ref[:, pl.ds(lane, LANES)] = ref[n, 0:slots, :]
            c_ref[:, pl.ds(lane, LANES)] = ref[n, slots : 2 * slots, :]


def lanes_of(refs, side, out_ref):
    at = 0
    for ref in refs:
        rows = ref.shape[0]
        for y in range(ref.shape[1] // (2 * LANES)):
            lane = pl.multiple_of((2 * y + side) * LANES, LANES)
            out_ref[at : at + rows, y * LANES : (y + 1) * LANES] = ref[:, pl.ds(lane, LANES)]
        at += rows


def expert_kernel(
    extra, at_ref, own_ref, other_ref, gate_ref, up_ref, down_ref,
    send_ref, dots_ref, hidden_ref, joined_ref, x_ref, c_ref, half_ref,
):
    assemble(at_ref, own_ref, other_ref, x_ref, c_ref)
    slots = x_ref.shape[0]
    hidden, hidden_grad, d_gate, d_up = swiglu_back(
        x_ref[...], c_ref[...], gate_ref[...], up_ref[...], down_ref[...]
    )
    hidden_ref[...] = hidden
    joined = jnp.concatenate([d_gate, d_up], axis=0)
    joined_ref[...] = joined
    lanes_of((gate_ref, up_ref), 1 - (at_ref[0] & 1), half_ref)
    back = tn(joined, half_ref[...]).astype(BF)
    dots = jnp.sum(hidden.astype(F32) * hidden_grad, axis=0, keepdims=True)
    wide = up(slots, LANES)
    dots = jnp.concatenate([dots, jnp.zeros((1, wide - slots), F32)], axis=1)
    line = rows_of((extra, LANES))
    rest = jnp.zeros((extra, LANES), F32)
    for k in range(wide // LANES):
        rest = jnp.where(line == k, dots[:, k * LANES : (k + 1) * LANES], rest)
    rest = rest.astype(BF)
    dots_ref[...] = rest
    for y in range(send_ref.shape[0]):
        send_ref[y, 0:slots, :] = back[:, y * LANES : (y + 1) * LANES]
        send_ref[y, slots : slots + extra, :] = rest


def keep_kernel(at_ref, x_ref, joined_ref, gate_ref, up_ref, keep_ref, g_gate_ref, g_up_ref, squares_ref, half_ref):
    units, width = g_gate_ref.shape
    shares = width // LANES
    joined = joined_ref[...]
    lanes_of((gate_ref, up_ref), at_ref[0] & 1, half_ref)
    back = tn(joined, half_ref[...]).astype(BF)
    for y in range(keep_ref.shape[0]):
        keep_ref[y] = back[:, y * LANES : (y + 1) * LANES]
    line = rows_of((2 * shares, LANES))
    rest = jnp.zeros((2 * shares, LANES), F32)
    for k, out_ref in enumerate((g_gate_ref, g_up_ref)):
        g = nn(joined[k * units : (k + 1) * units, :], x_ref[...])
        out_ref[...] = g
        sums = jnp.sum(g * g, axis=0, keepdims=True)
        for p in range(shares):
            rest = jnp.where(line == k * shares + p, sums[:, p * LANES : (p + 1) * LANES], rest)
    squares_ref[...] = rest.astype(BF)


def add_kernel(keep_ref, taken_ref, dots_ref, squares_ref, out_ref):
    slots = keep_ref.shape[1]
    rows = taken_ref.shape[1]
    dots, squares = dots_ref[...].astype(F32), squares_ref[...]
    for y in range(out_ref.shape[0]):
        out_ref[y, 0:slots, :] = (keep_ref[y].astype(F32) + taken_ref[y, 0:slots, :].astype(F32)).astype(BF)
        out_ref[y, slots:rows, :] = (dots + taken_ref[y, slots:rows, :].astype(F32)).astype(BF)
        out_ref[y, rows : rows + squares.shape[0], :] = squares


def down_kernel(at_ref, own_ref, other_ref, hidden_ref, g_down_ref, n_down_ref, c_ref):
    assemble(at_ref, own_ref, other_ref, None, c_ref)
    g_down = nn(hidden_ref[...], c_ref[...])
    g_down_ref[...] = g_down
    units = g_down.shape[0]
    n_down = jnp.sum(g_down * g_down, axis=1, keepdims=True) * (1.0 / g_down.shape[1])
    same = rows_of((units, units)) == cols_of((units, units))
    n_down_ref[...] = jnp.sum(jnp.where(same, n_down, 0.0), axis=0, keepdims=True)


def return_kernel(cap, block, parts_ref, back_ref, squares_ref):
    size = back_ref.shape[0]
    slots = size // block * cap
    total = parts_ref[0].astype(F32)
    for y in range(1, parts_ref.shape[0]):
        total = total + parts_ref[y].astype(F32)
    squares_ref[...] = total[total.shape[0] - squares_ref.shape[0] :, :]
    row = rows_of((size, slots))
    slot = cols_of((size, slots))
    source = divided(row, block)
    inner = row - source * block
    mask = (slot == source * cap + inner) & (inner < cap)
    back = nn(picked(mask), total[0:slots, :].astype(BF))
    row = rows_of((size, LANES))
    source = divided(row, block)
    is_dot = row == source * block + cap
    for k in range(up(slots, LANES) // LANES):
        dots = total[slots + k : slots + k + 1, :].astype(BF).astype(F32)
        mine = divided(cols_of((size, LANES)) + k * LANES, cap) == source
        left = jnp.where(is_dot & mine, dots, 0.0).astype(BF)
        number = rows_of((LANES, LANES)) + k * LANES
        place = number - divided(number, cap) * cap
        back = back + nn(left, picked(place == cols_of((LANES, LANES))))
    back_ref[...] = back.astype(BF)


def shared_sum_kernel(parts_ref, grad_ref, norm_ref):
    total = parts_ref[0].astype(F32)
    for e in range(1, parts_ref.shape[0]):
        total = total + parts_ref[e].astype(F32)
    rows, width = grad_ref.shape
    count = width // LANES
    lane = cols_of(norm_ref.shape)
    norm = jnp.zeros(norm_ref.shape, F32)
    for i in range(rows):
        mine = total[i * count : (i + 1) * count, :]
        for p in range(count):
            grad_ref[i : i + 1, p * LANES : (p + 1) * LANES] = mine[p : p + 1, :]
        square = jnp.sum(jnp.sum(mine * mine, axis=0, keepdims=True), axis=1, keepdims=True)
        norm = jnp.where(lane == i, square * (1.0 / width), norm)
    norm_ref[...] = norm


def combine_kernel(cap, block, recv_ref, routes_ref, rank_ref, gates_ref, near_ref, far_ref, grad_ref, gate_grad_ref):
    size = recv_ref.shape[0]
    toks = routes_ref.shape[1]
    recv = recv_ref[...]
    row = rows_of((size, toks))
    lane = rows_of((LANES, toks))
    at = []
    for k in range(2):
        route, rank = routes_ref[k : k + 1, :], rank_ref[k : k + 1, :]
        at.append(row == route * block + rank)
        dots = tn(recv, picked(row == route * block + cap))
        dot = jnp.sum(jnp.where(lane == rank, dots, 0.0), axis=0, keepdims=True)
        gate_grad_ref[k : k + 1, :] = dot / gates_ref[k : k + 1, :]
    grad_ref[...] = (tn(picked(at[0] | at[1]), recv) + (near_ref[...] + far_ref[...].astype(F32))).astype(BF)


def local(body, args, outs, scratch=(), scalars=0, flops=2 * 10**9):
    specs = [pl.BlockSpec(memory_space=pltpu.SMEM)] * scalars
    specs = specs + [pl.BlockSpec(memory_space=pltpu.VMEM)] * (len(args) - scalars)
    return pl.pallas_call(
        body,
        in_specs=specs,
        out_shape=tuple(jax.ShapeDtypeStruct(s, d) for s, d in outs),
        out_specs=tuple(pl.BlockSpec(memory_space=pltpu.VMEM) for _ in outs),
        scratch_shapes=list(scratch),
        cost_estimate=pl.CostEstimate(flops=flops, bytes_accessed=flops // 500, transcendentals=0),
        compiler_params=pltpu.CompilerParams(vmem_limit_bytes=20 * 1024 * 1024),
    )(*args)


def shifted(x, by, count):
    return lax.ppermute(x, "y", [(i, (i + by) % count) for i in range(count)])


def all_steps(tokens, routes, route_gates, cotangent, w_gate, w_up, w_down, s_gate, s_up, s_down):
    tp = ("y", "core")
    ep_count = lax.axis_size("ep")
    shares = lax.axis_size(tp)
    chips = shares // 2
    at = lax.axis_index(tp).astype(jnp.int32).reshape(1)
    toks, width = tokens.shape
    units = w_gate.shape[2]
    cap = max(2, (9 * toks * 2 + 8 * ep_count - 1) // (8 * ep_count))
    slots = ep_count * cap
    back_block = up(cap + 1, 8)
    routes_t, gates_t = routes.T, route_gates.T

    narrow = [pl.BlockSpec((toks, LANES), lambda i, s, n=n: (0, lax.rem(s[0] + n * chips, shares))) for n in range(2)]
    whole = pl.BlockSpec((2, toks), lambda i, s: (0, 0))
    send, ranks = pl.pallas_call(
        functools.partial(dispatch_kernel, ep_count, cap),
        out_shape=(
            jax.ShapeDtypeStruct((4 * slots, LANES), BF),
            jax.ShapeDtypeStruct((2, toks), jnp.int32),
        ),
        grid_spec=pltpu.PrefetchScalarGridSpec(
            num_scalar_prefetch=1,
            grid=(1,),
            in_specs=[whole, whole] + narrow + narrow,
            out_specs=(
                pl.BlockSpec((4 * slots, LANES), lambda i, s: (0, 0)),
                pl.BlockSpec((2, toks), lambda i, s: (0, 0)),
            ),
        ),
    )(at, routes_t, gates_t, tokens, tokens, cotangent, cotangent)
    recv = lax.all_to_all(send.reshape(ep_count, 4 * cap, LANES), "ep", 0, 0, tiled=True)

    keep, give, term = local(
        shared_kernel,
        (at, tokens, cotangent, s_gate.T, s_up.T, s_down),
        [((chips, toks, LANES), BF)] * 2 + [((ep_count, units * shares // ep_count, LANES), BF)],
        [pltpu.VMEM((units, shares, LANES), F32), pltpu.VMEM((shares, toks, LANES), BF)],
        scalars=1,
        flops=4 * 10**9,
    )
    swap = [(0, 1), (1, 0)]
    taken = lax.ppermute(give, "core", swap)
    recv, keep, taken, term = lax.optimization_barrier((recv, keep, taken, term))
    term_parts = lax.all_to_all(term, "ep", 0, 0, tiled=True)

    near, far = 4 * slots, 2 * slots
    go_up, go_down, go_far_up, go_far_down, stay = local(
        functools.partial(compact_kernel, cap),
        (recv.reshape(4 * slots, LANES), keep, taken),
        [((near + 2 * toks, LANES), BF)] * 2 + [((far + toks, LANES), BF)] * 2 + [((2, toks, LANES), F32)],
    )
    came_up = shifted(go_up, 1, chips)
    came_down = shifted(go_down, -1, chips)
    came_far_up = shifted(go_far_up, 2, chips)
    came_far_down = shifted(go_far_down, -2, chips)
    own, shared_near, shared_far = local(
        join_kernel,
        (go_up, came_up, came_down, came_far_up, came_far_down, stay),
        [((chips, far, LANES), BF), ((toks, LANES), F32), ((toks, LANES), BF)],
    )
    other = lax.ppermute(own, "core", swap)
    shared_far = shifted(shared_far, chips // 2, chips)

    extra = up(up(slots, LANES) // LANES, 16)
    weights = (w_gate[0].T, w_up[0].T)
    half = pltpu.VMEM((2 * units, width // 2), BF)
    give, dots, hidden, joined, x = local(
        functools.partial(expert_kernel, extra),
        (at, own, other, *weights, w_down[0]),
        [
            ((chips, slots + extra, LANES), BF),
            ((extra, LANES), BF),
            ((units, slots), BF),
            ((2 * units, slots), BF),
            ((slots, width), BF),
        ],
        [pltpu.VMEM((slots, width), BF), half],
        scalars=1,
        flops=6 * 10**9,
    )
    taken = lax.ppermute(give, "core", swap)
    grads = ((units, width), F32)
    keep, g_gate, g_up, squares = local(
        keep_kernel,
        (at, x, joined, *weights),
        [((chips, slots, LANES), BF), grads, grads, ((2 * shares, LANES), BF)],
        [half],
        scalars=1,
        flops=4 * 10**9,
    )
    (pair,) = local(
        add_kernel, (keep, taken, dots, squares), [((chips, slots + extra + 2 * shares, LANES), BF)]
    )
    pair_parts = lax.all_to_all(pair, "y", 0, 0, tiled=True)

    g_down, n_down = local(
        down_kernel,
        (at, own, other, hidden),
        [grads, ((1, units), F32)],
        [pltpu.VMEM((slots, width), BF)],
        scalars=1,
        flops=3 * 10**9,
    )
    back, squares = local(
        functools.partial(return_kernel, cap, back_block),
        (pair_parts,),
        [((ep_count * back_block, LANES), BF), ((2 * shares, LANES), F32)],
    )
    squares = squares + lax.ppermute(squares, "core", swap)
    norm_in = (squares * (1.0 / (units * shares))).reshape(2, width)
    came = lax.all_to_all(back.reshape(ep_count, back_block, LANES), "ep", 0, 0, tiled=True)
    token_grad, gate_grad = local(
        functools.partial(combine_kernel, cap, back_block),
        (came.reshape(ep_count * back_block, LANES), routes_t, ranks, gates_t, shared_near, shared_far),
        [((toks, LANES), BF), ((2, toks), F32)],
    )

    grad_shared, norm_shared = local(
        shared_sum_kernel, (term_parts,), [((term.shape[1] * LANES // width, width), F32), ((1, LANES), F32)]
    )
    norm_shared = norm_shared[0, : grad_shared.shape[0]]
    return (
        token_grad,
        gate_grad.T,
        g_gate.T[None],
        g_up.T[None],
        g_down[None],
        grad_shared,
        norm_in[None],
        n_down,
        norm_shared,
    )


def solution(mesh):
    tp = ("y", "core")
    ep_count, tp_count = mesh.devices.shape
    fine = Mesh(mesh.devices.reshape(ep_count, tp_count // 2, 2), ("ep", "y", "core"))
    placed = (
        P("ep", None),
        P("ep", None),
        P("ep", None),
        P("ep", None),
        P("ep", None, tp),
        P("ep", None, tp),
        P("ep", tp, None),
        P(None, tp),
        P(None, tp),
        P(tp, None),
    )
    return jax.shard_map(
        all_steps,
        mesh=fine,
        in_specs=placed,
        out_specs=(
            P("ep", tp),
            P("ep", None),
            P("ep", None, tp),
            P("ep", None, tp),
            P("ep", tp, None),
            P(("y", "core", "ep"), None),
            P("ep", None, None),
            P("ep", tp),
            P(("y", "core", "ep")),
        ),
        check_vma=False,
    )
```

time: 154 us -> 141 us (0.916); the launches traced: 154 us -> 139 us
  waiting for transfers between devices: 71.7 us -> 46.3 us
  starting transfers between devices: 58.6 us -> 72.8 us
  other arithmetic: 5.55 us -> 0.01 us
  local copies, waits for them, and re-layouts: 1.7 us -> 3.79 us
    all_to_all x1, waiting for transfers between devices: 23.4 us -> 10.3 us  [all_steps(): pair_parts = lax.all_to_all(pair, 'y', 0, 0, tiled=True)]
    ppermute x4 -> x5, starting transfers between devices: 13.3 us -> 21.7 us  [shifted(): return lax.ppermute(x, 'y', [(i, (i + by) % count) for i in range(count)])]
    all_to_all x1, waiting for transfers between devices: 17.6 us -> 10.2 us  [all_steps(): term_parts = lax.all_to_all(term, 'ep', 0, 0, tiled=True)]
    all_to_all x1, waiting for transfers between devices: 14.5 us -> 11.2 us  [all_steps(): lax.all_to_all(send.reshape(ep_count, 4 * cap, LANES), 'ep', 0, 0, tiled=...]
    ppermute x0 -> x1, starting transfers between devices: none -> 2.81 us  [all_steps(): squares = squares + lax.ppermute(squares, 'core', swap)]
    ppermute x1 -> x2, starting transfers between devices: 2.28 us -> 5.05 us  [all_steps(): taken = lax.ppermute(give, 'core', swap)]
    convert_element_type x1 -> x0, other arithmetic: 2.45 us -> none  [all_steps(): pair = (keep.astype(F32) + taken.astype(F32)).astype(BF)]
    ppermute x1, waiting for transfers between devices: 2.37 us -> 0.01 us  [all_steps(): other = lax.ppermute(own, 'core', swap)]
  transfers between devices with their start and end apart: 10 -> 13, of which waited for: 7 -> 7; matrix products, arithmetic and copies ran while one was open for 4% -> 1% of each run, Pallas kernels for 3% -> 8%
where the time goes in v2:
time: 141 us; the launch traced here: 139 us
  starting transfers between devices  72.8 us (52%)
  waiting for transfers between devices  46.3 us (33%)
  Pallas kernels  15 us (11%)
  local copies, waits for them, and re-layouts  3.79 us (3%)
    ppermute x5, starting transfers between devices, shifted(): return lax.ppermute(x, 'y', [(i, (i + by) % count) for i in range(count)])  21.7 us
    all_to_all x1, starting transfers between devices, all_steps(): lax.all_to_all(send.reshape(ep_count, 4 * cap, LANES), 'ep', 0, 0, tiled=...  18.8 us
    pallas_call x10, Pallas kernels, local(): pl.pallas_call(body, in_specs=specs, out_shape=tuple((jax.ShapeDtypeStruc...  12.6 us
    all_to_all x1, waiting for transfers between devices, all_steps(): lax.all_to_all(send.reshape(ep_count, 4 * cap, LANES), 'ep', 0, 0, tiled=...  11.2 us
    all_to_all x1, waiting for transfers between devices, all_steps(): pair_parts = lax.all_to_all(pair, 'y', 0, 0, tiled=True)  10.3 us
    all_to_all x1, waiting for transfers between devices, all_steps(): term_parts = lax.all_to_all(term, 'ep', 0, 0, tiled=True)  10.2 us
    all_to_all x1, starting transfers between devices, all_steps(): lax.all_to_all(back.reshape(ep_count, back_block, LANES), 'ep', 0, 0, til...  8.15 us
    ppermute x5, waiting for transfers between devices, shifted(): return lax.ppermute(x, 'y', [(i, (i + by) % count) for i in range(count)])  7.26 us
  transfers between devices with their start and end apart: 13, of which 7 were waited for; matrix products, arithmetic and copies ran while one was open for 1% of the time, Pallas kernels for 8%

profile of v2, /device:TPU:1, one launch (start us, length us, event | category | flops | bytes accessed | tf_op | source)
XLA Modules:
  0.0 138.9 jit_solution(9368807173371660263)
XLA Ops:
  0.7 2.4 %shard_map.169 = (bf16[1152,128]{1,0:T(8,128)(2,1)}, s32[2,128]{1,0:T(2,128)}) custom-call(s32[1]{0:T(128)} %bitcast.share_ref.at_ref, s32[2,128]{1,0:T(2,128)} %bitcast.28, f32[2,128]{1,0:T(2,128)} %bitcast.30, bf16[128,2048]{1,0:T(8,128)(2,1)} %tok_ref.1, bf16[128,2048]{1,0:T(8,128)(2,1)} %tok_ref.1, bf16[128,2048]{1,0:T(8,128)(2,1)} %cot_ref.1, ...), custom_call_target="tpu_custom_call" | custom-call | tf_op jit(solution)/shard_map/pallas_call | solution.py:357
  3.1 18.8 %all-to-all-start = ((bf16[48,24,128]{2,1,0:T(8,128)(2,1)}), bf16[48,24,128]{2,1,0:T(8,128)(2,1)S(1)}, u32[]{:S(2)}, u32[]{:S(2)}) async-start(bf16[48,24,128]{2,1,0:T(8,128)(2,1)} %bitcast.39), calls=%async_computation | async-start | bytes 589824 | tf_op jit(solution)/shard_map/all_to_all | solution.py:373
  21.9 0.0 copy-done
  21.9 0.0 copy-done.1
  22.0 2.3 %shard_map.170 = (bf16[8,128,128]{2,1,0:T(8,128)(2,1)S(1)}, bf16[8,128,128]{2,1,0:T(8,128)(2,1)S(1)}, bf16[48,32,128]{2,1,0:T(8,128)(2,1)}) custom-call(s32[1]{0:T(128)} %bitcast.share_ref.at_ref, bf16[128,2048]{1,0:T(8,128)(2,1)S(1)} %copy-done, bf16[128,2048]{1,0:T(8,128)(2,1)S(1)} %copy-done.1, bf16[96,2048]{1,0:T(8,128)(2,1)S(1)} %bitcast.32, ...), custom_call_target="tpu_custom_call" | custom-call | flops 4000000000 | bytes 8000000 | tf_op jit(solution)/shard_map/pallas_call | solution.py:327
  24.3 2.9 %collective-permute-start = (bf16[8,128,128]{2,1,0:T(8,128)(2,1)S(1)}, bf16[8,128,128]{2,1,0:T(8,128)(2,1)S(1)}, u32[]{:S(2)}, u32[]{:S(2)}) collective-permute-start(bf16[8,128,128]{2,1,0:T(8,128)(2,1)S(1)} %get-tuple-element.45), channel_id=1, source_target_pairs={{0,1},{1,0},{2,3},{3,2},{4,5},{5,4},{6,7},{7,6},{8,9},{9,8},{10,11... | collective-permute-start | bytes 786440 | tf_op jit(solution)/shard_map/ppermute | solution.py:384
  27.2 1.1 collective-permute-done.taken_ref
  28.3 11.2 %all-to-all-done = bf16[48,24,128]{2,1,0:T(8,128)(2,1)S(1)} async-done(((bf16[48,24,128]{2,1,0:T(8,128)(2,1)}), bf16[48,24,128]{2,1,0:T(8,128)(2,1)S(1)}, u32[]{:S(2)}, u32[]{:S(2)}) %all-to-all-start) | async-done | bytes 294944 | tf_op jit(solution)/shard_map/all_to_all | solution.py:373
  39.5 0.3 shard_map.171
  39.8 5.1 %collective-permute-start.2 = (bf16[1408,128]{1,0:T(8,128)(2,1)S(1)}, bf16[1408,128]{1,0:T(8,128)(2,1)S(1)}, u32[]{:S(2)}, u32[]{:S(2)}) collective-permute-start(bf16[1408,128]{1,0:T(8,128)(2,1)S(1)} %get-tuple-element.51), channel_id=1, source_target_pairs={{0,14},{2,0},{4,2},{6,4},{8,6},{10,8},{12,10},{14,12},{1,15},{3,1}... | collective-permute-start | bytes 1081352 | tf_op jit(solution)/shard_map/ppermute | solution.py:339
  45.0 1.9 %collective-permute-start.1 = (bf16[1408,128]{1,0:T(8,128)(2,1)S(1)}, bf16[1408,128]{1,0:T(8,128)(2,1)S(1)}, u32[]{:S(2)}, u32[]{:S(2)}) collective-permute-start(bf16[1408,128]{1,0:T(8,128)(2,1)S(1)} %get-tuple-element.50.mine_ref), channel_id=1, source_target_pairs={{0,2},{2,4},{4,6},{6,8},{8,10},{10,12},{12,14},{14,0},{1,3},{3,5},... | collective-permute-start | bytes 1081352 | tf_op jit(solution)/shard_map/ppermute | solution.py:339
  46.9 2.5 %collective-permute-start.3 = (bf16[704,128]{1,0:T(8,128)(2,1)S(1)}, bf16[704,128]{1,0:T(8,128)(2,1)S(1)}, u32[]{:S(2)}, u32[]{:S(2)}) collective-permute-start(bf16[704,128]{1,0:T(8,128)(2,1)S(1)} %get-tuple-element.52), channel_id=1, source_target_pairs={{0,4},{2,6},{4,8},{6,10},{8,12},{10,14},{12,0},{14,2},{1,5},{3,7},... | collective-permute-start | bytes 540680 | tf_op jit(solution)/shard_map/ppermute | solution.py:339
  49.4 4.9 %collective-permute-start.4 = (bf16[704,128]{1,0:T(8,128)(2,1)S(1)}, bf16[704,128]{1,0:T(8,128)(2,1)S(1)}, u32[]{:S(2)}, u32[]{:S(2)}) collective-permute-start(bf16[704,128]{1,0:T(8,128)(2,1)S(1)} %get-tuple-element.53), channel_id=1, source_target_pairs={{0,12},{2,14},{4,0},{6,2},{8,4},{10,6},{12,8},{14,10},{1,13},{3,15... | collective-permute-start | bytes 540680 | tf_op jit(solution)/shard_map/ppermute | solution.py:339
  54.3 6.1 %collective-permute-done.3.far_up_ref = bf16[704,128]{1,0:T(8,128)(2,1)S(1)} collective-permute-done((bf16[704,128]{1,0:T(8,128)(2,1)S(1)}, bf16[704,128]{1,0:T(8,128)(2,1)S(1)}, u32[]{:S(2)}, u32[]{:S(2)}) %collective-permute-start.3) | collective-permute-done | bytes 180256 | tf_op jit(solution)/shard_map/ppermute | solution.py:339
  60.4 1.2 collective-permute-done.4.far_down_ref
  61.5 0.0 collective-permute-done.2.down_ref
  61.5 0.0 collective-permute-done.1.up_ref
  61.6 0.1 shard_map.172
  61.7 0.6 copy-done.12
  62.3 5.5 %collective-permute-start.5 = (bf16[8,576,128]{2,1,0:T(8,128)(2,1)S(1)}, bf16[8,576,128]{2,1,0:T(8,128)(2,1)S(1)}, u32[]{:S(2)}, u32[]{:S(2)}) collective-permute-start(bf16[8,576,128]{2,1,0:T(8,128)(2,1)S(1)} %get-tuple-element.55.own_ref), channel_id=1, source_target_pairs={{0,1},{1,0},{2,3},{3,2},{4,5},{5,4},{6,7},{7,6},{8,9},{9,8},{10,11... | collective-permute-start | bytes 3538952 | tf_op jit(solution)/shard_map/ppermute | solution.py:403
  67.8 5.1 %all-to-all-start.3 = ((bf16[48,32,128]{2,1,0:T(8,128)(2,1)}), bf16[48,32,128]{2,1,0:T(8,128)(2,1)S(1)}, u32[]{:S(2)}, u32[]{:S(2)}) async-start(bf16[48,32,128]{2,1,0:T(8,128)(2,1)} %get-tuple-element.72), calls=%async_computation.3 | async-start | bytes 786432 | tf_op jit(solution)/shard_map/all_to_all | solution.py:386
  72.9 0.0 collective-permute-done.5.other_ref
  72.9 0.0 copy-start.8
  72.9 1.0 copy-done.8
  73.9 1.0 copy-done.10
  74.9 2.5 %shard_map.173 = (bf16[8,304,128]{2,1,0:T(8,128)(2,1)S(1)}, bf16[16,128]{1,0:T(8,128)(2,1)S(1)}, bf16[96,288]{1,0:T(8,128)(2,1)S(1)}, bf16[192,288]{1,0:T(8,128)(2,1)S(1)}, bf16[288,2048]{1,0:T(8,128)(2,1)S(1)}) custom-call(s32[1]{0:T(128)} %bitcast.share_ref.at_ref, bf16[8,576,128]{2,1,0:T(8,128)(2,1)S(1)} %get-tuple-element.55.own_ref, ...), custom_call_target="tpu_custom_call" | custom-call | flops 6000000000 | bytes 12000000 | tf_op jit(solution)/shard_map/pallas_call | solution.py:327
  77.5 2.2 %collective-permute-start.6 = (bf16[8,304,128]{2,1,0:T(8,128)(2,1)S(1)}, bf16[8,304,128]{2,1,0:T(8,128)(2,1)S(1)}, u32[]{:S(2)}, u32[]{:S(2)}) collective-permute-start(bf16[8,304,128]{2,1,0:T(8,128)(2,1)S(1)} %get-tuple-element.59), channel_id=1, source_target_pairs={{0,1},{1,0},{2,3},{3,2},{4,5},{5,4},{6,7},{7,6},{8,9},{9,8},{10,11... | collective-permute-start | bytes 1867784 | tf_op jit(solution)/shard_map/ppermute | solution.py:423
  79.7 2.0 %shard_map.174 = (bf16[8,288,128]{2,1,0:T(8,128)(2,1)S(1)}, f32[96,2048]{1,0:T(8,128)}, f32[96,2048]{1,0:T(8,128)}, bf16[32,128]{1,0:T(8,128)(2,1)S(1)}) custom-call(s32[1]{0:T(128)} %bitcast.share_ref.at_ref, bf16[288,2048]{1,0:T(8,128)(2,1)S(1)} %get-tuple-element.56.x_ref, bf16[192,288]{1,0:T(8,128)(2,1)S(1)} %get-tuple-element.57.joined_ref, ...), custom_call_target="tpu_custom_call" | custom-call | flops 4000000000 | bytes 8000000 | tf_op jit(solution)/shard_map/pallas_call | solution.py:327
  81.7 0.0 collective-permute-done.6.taken_ref
  81.7 1.0 shard_map.175
  82.7 10.2 %all-to-all-done.3.parts_ref = bf16[48,32,128]{2,1,0:T(8,128)(2,1)S(1)} async-done(((bf16[48,32,128]{2,1,0:T(8,128)(2,1)}), bf16[48,32,128]{2,1,0:T(8,128)(2,1)S(1)}, u32[]{:S(2)}, u32[]{:S(2)}) %all-to-all-start.3) | async-done | bytes 393248 | tf_op jit(solution)/shard_map/all_to_all | solution.py:386
  92.8 5.7 %all-to-all-start.1 = ((bf16[8,336,128]{2,1,0:T(8,128)(2,1)}), bf16[8,336,128]{2,1,0:T(8,128)(2,1)S(1)}, u32[]{:S(2)}, u32[]{:S(2)}) async-start(bf16[8,336,128]{2,1,0:T(8,128)(2,1)} %shard_map.175), calls=%async_computation.1 | async-start | bytes 1376256 | tf_op jit(solution)/shard_map/all_to_all | solution.py:436
  98.6 7.3 %collective-permute-start.7 = (bf16[128,128]{1,0:T(8,128)(2,1)S(1)}, bf16[128,128]{1,0:T(8,128)(2,1)S(1)}, u32[]{:S(2)}, u32[]{:S(2)}) collective-permute-start(bf16[128,128]{1,0:T(8,128)(2,1)S(1)} %get-tuple-element.65), channel_id=1, source_target_pairs={{0,8},{2,10},{4,12},{6,14},{8,0},{10,2},{12,4},{14,6},{1,9},{3,11}... | collective-permute-start | bytes 98312 | tf_op jit(solution)/shard_map/ppermute | solution.py:339
  105.8 0.7 shard_map.179
  106.5 0.5 slice_bitcast_fusion
  107.0 10.3 %all-to-all-done.1.parts_ref = bf16[8,336,128]{2,1,0:T(8,128)(2,1)S(1)} async-done(((bf16[8,336,128]{2,1,0:T(8,128)(2,1)}), bf16[8,336,128]{2,1,0:T(8,128)(2,1)S(1)}, u32[]{:S(2)}, u32[]{:S(2)}) %all-to-all-start.1) | async-done | bytes 688160 | tf_op jit(solution)/shard_map/all_to_all | solution.py:436
  117.3 1.1 shard_map.176
  118.4 8.1 %all-to-all-start.2 = ((bf16[48,8,128]{2,1,0:T(8,128)(2,1)}), bf16[48,8,128]{2,1,0:T(8,128)(2,1)S(1)}, u32[]{:S(2)}, u32[]{:S(2)}) async-start(bf16[48,8,128]{2,1,0:T(8,128)(2,1)} %bitcast.12), calls=%async_computation.2 | async-start | bytes 196608 | tf_op jit(solution)/shard_map/all_to_all | solution.py:453
  126.6 2.8 %collective-permute-start.8 = (f32[32,128]{1,0:T(8,128)S(1)}, f32[32,128]{1,0:T(8,128)S(1)}, u32[]{:S(2)}, u32[]{:S(2)}) collective-permute-start(f32[32,128]{1,0:T(8,128)S(1)} %get-tuple-element.74), channel_id=1, source_target_pairs={{0,1},{1,0},{2,3},{3,2},{4,5},{5,4},{6,7},{7,6},{8,9},{9,8},{10,11... | collective-permute-start | bytes 49160 | tf_op jit(solution)/shard_map/ppermute | solution.py:451
  129.4 0.0 copy-start.2
  129.4 0.0 copy-start.3
  129.4 0.0 copy-start.11
  129.4 1.6 %shard_map.178 = (f32[96,2048]{1,0:T(8,128)}, f32[1,96]{1,0:T(1,128)}) custom-call(s32[1]{0:T(128)} %bitcast.share_ref.at_ref, bf16[8,576,128]{2,1,0:T(8,128)(2,1)S(1)} %get-tuple-element.55.own_ref, bf16[8,576,128]{2,1,0:T(8,128)(2,1)S(1)} %collective-permute-done.5.other_ref, bf16[96,288]{1,0:T(8,128)(2,1)S(1)} %copy-done.15), custom_call_target="tpu_custom_call" | custom-call | flops 3000000000 | bytes 6000000 | tf_op jit(solution)/shard_map/pallas_call | solution.py:327
  131.1 0.0 collective-permute-done.8
  131.1 0.6 broadcast_in_dim_reshape.3
  131.7 0.0 collective-permute-done.7.far_ref
  131.7 6.2 %all-to-all-done.2 = bf16[48,8,128]{2,1,0:T(8,128)(2,1)S(1)} async-done(((bf16[48,8,128]{2,1,0:T(8,128)(2,1)}), bf16[48,8,128]{2,1,0:T(8,128)(2,1)S(1)}, u32[]{:S(2)}, u32[]{:S(2)}) %all-to-all-start.2) | async-done | bytes 98336 | tf_op jit(solution)/shard_map/all_to_all | solution.py:453
  138.0 0.9 shard_map.177
  (24 shorter events, 0.1 us)
Async XLA Ops:
  0.6 21.3 %copy-start = (bf16[128,2048]{1,0:T(8,128)(2,1)S(1)}, bf16[128,2048]{1,0:T(8,128)(2,1)}, u32[]{:S(2)}) copy-start(bf16[128,2048]{1,0:T(8,128)(2,1)} %tok_ref.1) | copy-start | bytes 1572868
  0.7 21.3 %copy-start.1 = (bf16[128,2048]{1,0:T(8,128)(2,1)S(1)}, bf16[128,2048]{1,0:T(8,128)(2,1)}, u32[]{:S(2)}) copy-start(bf16[128,2048]{1,0:T(8,128)(2,1)} %cot_ref.1) | copy-start | bytes 1572868
  0.7 21.3 %copy-start.4 = (bf16[2048,96]{0,1:T(8,128)(2,1)S(1)}, bf16[2048,96]{0,1:T(8,128)(2,1)}, u32[]{:S(2)}) copy-start(bf16[2048,96]{0,1:T(8,128)(2,1)} %param.17) | copy-start | bytes 1179652
  0.7 21.3 %copy-start.5 = (bf16[2048,96]{0,1:T(8,128)(2,1)S(1)}, bf16[2048,96]{0,1:T(8,128)(2,1)}, u32[]{:S(2)}) copy-start(bf16[2048,96]{0,1:T(8,128)(2,1)} %param.18) | copy-start | bytes 1179652
  0.7 21.3 %copy-start.6 = (bf16[96,2048]{1,0:T(8,128)(2,1)S(1)}, bf16[96,2048]{1,0:T(8,128)(2,1)}, u32[]{:S(2)}) copy-start(bf16[96,2048]{1,0:T(8,128)(2,1)} %down_ref.1) | copy-start | bytes 1179652
  3.1 36.4 %all-to-all-start = ((bf16[48,24,128]{2,1,0:T(8,128)(2,1)}), bf16[48,24,128]{2,1,0:T(8,128)(2,1)S(1)}, u32[]{:S(2)}, u32[]{:S(2)}) async-start(bf16[48,24,128]{2,1,0:T(8,128)(2,1)} %bitcast.39), calls=%async_computation | async-start | bytes 589824 | tf_op jit(solution)/shard_map/all_to_all | solution.py:373
  24.3 4.0 %collective-permute-start = (bf16[8,128,128]{2,1,0:T(8,128)(2,1)S(1)}, bf16[8,128,128]{2,1,0:T(8,128)(2,1)S(1)}, u32[]{:S(2)}, u32[]{:S(2)}) collective-permute-start(bf16[8,128,128]{2,1,0:T(8,128)(2,1)S(1)} %get-tuple-element.45), channel_id=1, source_target_pairs={{0,1},{1,0},{2,3},{3,2},{4,5},{5,4},{6,7},{7,6},{8,9},{9,8},{10,11... | collective-permute-start | bytes 786440 | tf_op jit(solution)/shard_map/ppermute | solution.py:384
  39.8 21.7 %collective-permute-start.2 = (bf16[1408,128]{1,0:T(8,128)(2,1)S(1)}, bf16[1408,128]{1,0:T(8,128)(2,1)S(1)}, u32[]{:S(2)}, u32[]{:S(2)}) collective-permute-start(bf16[1408,128]{1,0:T(8,128)(2,1)S(1)} %get-tuple-element.51), channel_id=1, source_target_pairs={{0,14},{2,0},{4,2},{6,4},{8,6},{10,8},{12,10},{14,12},{1,15},{3,1}... | collective-permute-start | bytes 1081352 | tf_op jit(solution)/shard_map/ppermute | solution.py:339
  45.0 16.6 %collective-permute-start.1 = (bf16[1408,128]{1,0:T(8,128)(2,1)S(1)}, bf16[1408,128]{1,0:T(8,128)(2,1)S(1)}, u32[]{:S(2)}, u32[]{:S(2)}) collective-permute-start(bf16[1408,128]{1,0:T(8,128)(2,1)S(1)} %get-tuple-element.50.mine_ref), channel_id=1, source_target_pairs={{0,2},{2,4},{4,6},{6,8},{8,10},{10,12},{12,14},{14,0},{1,3},{3,5},... | collective-permute-start | bytes 1081352 | tf_op jit(solution)/shard_map/ppermute | solution.py:339
  46.9 13.5 %collective-permute-start.3 = (bf16[704,128]{1,0:T(8,128)(2,1)S(1)}, bf16[704,128]{1,0:T(8,128)(2,1)S(1)}, u32[]{:S(2)}, u32[]{:S(2)}) collective-permute-start(bf16[704,128]{1,0:T(8,128)(2,1)S(1)} %get-tuple-element.52), channel_id=1, source_target_pairs={{0,4},{2,6},{4,8},{6,10},{8,12},{10,14},{12,0},{14,2},{1,5},{3,7},... | collective-permute-start | bytes 540680 | tf_op jit(solution)/shard_map/ppermute | solution.py:339
  49.4 12.2 %collective-permute-start.4 = (bf16[704,128]{1,0:T(8,128)(2,1)S(1)}, bf16[704,128]{1,0:T(8,128)(2,1)S(1)}, u32[]{:S(2)}, u32[]{:S(2)}) collective-permute-start(bf16[704,128]{1,0:T(8,128)(2,1)S(1)} %get-tuple-element.53), channel_id=1, source_target_pairs={{0,12},{2,14},{4,0},{6,2},{8,4},{10,6},{12,8},{14,10},{1,13},{3,15... | collective-permute-start | bytes 540680 | tf_op jit(solution)/shard_map/ppermute | solution.py:339
  61.5 11.4 %copy-start.7 = (bf16[1,96,2048]{2,1,0:T(8,128)(2,1)S(1)}, bf16[1,96,2048]{2,1,0:T(8,128)(2,1)}, u32[]{:S(2)}) copy-start(bf16[1,96,2048]{2,1,0:T(8,128)(2,1)} %param.16) | copy-start | bytes 1179652
  61.7 0.6 copy-start.12
  62.3 10.6 %collective-permute-start.5 = (bf16[8,576,128]{2,1,0:T(8,128)(2,1)S(1)}, bf16[8,576,128]{2,1,0:T(8,128)(2,1)S(1)}, u32[]{:S(2)}, u32[]{:S(2)}) collective-permute-start(bf16[8,576,128]{2,1,0:T(8,128)(2,1)S(1)} %get-tuple-element.55.own_ref), channel_id=1, source_target_pairs={{0,1},{1,0},{2,3},{3,2},{4,5},{5,4},{6,7},{7,6},{8,9},{9,8},{10,11... | collective-permute-start | bytes 3538952 | tf_op jit(solution)/shard_map/ppermute | solution.py:403
  67.8 25.0 %all-to-all-start.3 = ((bf16[48,32,128]{2,1,0:T(8,128)(2,1)}), bf16[48,32,128]{2,1,0:T(8,128)(2,1)S(1)}, u32[]{:S(2)}, u32[]{:S(2)}) async-start(bf16[48,32,128]{2,1,0:T(8,128)(2,1)} %get-tuple-element.72), calls=%async_computation.3 | async-start | bytes 786432 | tf_op jit(solution)/shard_map/all_to_all | solution.py:386
  72.9 1.0 copy-start.8
  73.9 1.0 copy-start.10
  74.9 4.8 %copy-start.9 = (bf16[1,2048,96]{1,2,0:T(8,128)(2,1)S(1)}, bf16[1,2048,96]{1,2,0:T(8,128)(2,1)}, u32[]{:S(2)}) copy-start(bf16[1,2048,96]{1,2,0:T(8,128)(2,1)} %param.14) | copy-start | bytes 1179652
  77.5 4.2 %copy-start.14 = (bf16[96,288]{1,0:T(8,128)(2,1)}, bf16[96,288]{1,0:T(8,128)(2,1)S(1)}, u32[]{:S(2)}) copy-start(bf16[96,288]{1,0:T(8,128)(2,1)S(1)} %get-tuple-element.70.hidden_ref) | copy-start | bytes 165892
  77.5 4.2 %collective-permute-start.6 = (bf16[8,304,128]{2,1,0:T(8,128)(2,1)S(1)}, bf16[8,304,128]{2,1,0:T(8,128)(2,1)S(1)}, u32[]{:S(2)}, u32[]{:S(2)}) collective-permute-start(bf16[8,304,128]{2,1,0:T(8,128)(2,1)S(1)} %get-tuple-element.59), channel_id=1, source_target_pairs={{0,1},{1,0},{2,3},{3,2},{4,5},{5,4},{6,7},{7,6},{8,9},{9,8},{10,11... | collective-permute-start | bytes 1867784 | tf_op jit(solution)/shard_map/ppermute | solution.py:423
  92.8 24.4 %all-to-all-start.1 = ((bf16[8,336,128]{2,1,0:T(8,128)(2,1)}), bf16[8,336,128]{2,1,0:T(8,128)(2,1)S(1)}, u32[]{:S(2)}, u32[]{:S(2)}) async-start(bf16[8,336,128]{2,1,0:T(8,128)(2,1)} %shard_map.175), calls=%async_computation.1 | async-start | bytes 1376256 | tf_op jit(solution)/shard_map/all_to_all | solution.py:436
  98.6 33.2 %collective-permute-start.7 = (bf16[128,128]{1,0:T(8,128)(2,1)S(1)}, bf16[128,128]{1,0:T(8,128)(2,1)S(1)}, u32[]{:S(2)}, u32[]{:S(2)}) collective-permute-start(bf16[128,128]{1,0:T(8,128)(2,1)S(1)} %get-tuple-element.65), channel_id=1, source_target_pairs={{0,8},{2,10},{4,12},{6,14},{8,0},{10,2},{12,4},{14,6},{1,9},{3,11}... | collective-permute-start | bytes 98312 | tf_op jit(solution)/shard_map/ppermute | solution.py:339
  107.0 22.4 %copy-start.15 = (bf16[96,288]{1,0:T(8,128)(2,1)S(1)}, bf16[96,288]{1,0:T(8,128)(2,1)}, u32[]{:S(2)}) copy-start(bf16[96,288]{1,0:T(8,128)(2,1)} %copy-done.14) | copy-start | bytes 165892
  118.4 19.5 %all-to-all-start.2 = ((bf16[48,8,128]{2,1,0:T(8,128)(2,1)}), bf16[48,8,128]{2,1,0:T(8,128)(2,1)S(1)}, u32[]{:S(2)}, u32[]{:S(2)}) async-start(bf16[48,8,128]{2,1,0:T(8,128)(2,1)} %bitcast.12), calls=%async_computation.2 | async-start | bytes 196608 | tf_op jit(solution)/shard_map/all_to_all | solution.py:453
  126.6 4.5 %collective-permute-start.8 = (f32[32,128]{1,0:T(8,128)S(1)}, f32[32,128]{1,0:T(8,128)S(1)}, u32[]{:S(2)}, u32[]{:S(2)}) collective-permute-start(f32[32,128]{1,0:T(8,128)S(1)} %get-tuple-element.74), channel_id=1, source_target_pairs={{0,1},{1,0},{2,3},{3,2},{4,5},{5,4},{6,7},{7,6},{8,9},{9,8},{10,11... | collective-permute-start | bytes 49160 | tf_op jit(solution)/shard_map/ppermute | solution.py:451
  129.4 8.6 %copy-start.2 = (s32[128,2]{0,1:T(2,128)S(1)}, s32[128,2]{0,1:T(2,128)}, u32[]{:S(2)}) copy-start(s32[128,2]{0,1:T(2,128)} %param.11) | copy-start | bytes 3076
  129.4 8.6 %copy-start.3 = (f32[128,2]{0,1:T(2,128)S(1)}, f32[128,2]{0,1:T(2,128)}, u32[]{:S(2)}) copy-start(f32[128,2]{0,1:T(2,128)} %param.12) | copy-start | bytes 3076
  129.4 8.5 %copy-start.11 = (s32[2,128]{1,0:T(2,128)S(1)}, s32[2,128]{1,0:T(2,128)}, u32[]{:S(2)}) copy-start(s32[2,128]{1,0:T(2,128)} %get-tuple-element.63.rank_ref) | copy-start | bytes 3076
  129.4 8.5 %copy-start.13 = (f32[128,128]{1,0:T(8,128)S(1)}, f32[128,128]{1,0:T(8,128)}, u32[]{:S(2)}) copy-start(f32[128,128]{1,0:T(8,128)} %copy-done.12) | copy-start | bytes 196612

commit v3 on v2

--- a/solution.py
+++ b/solution.py
@@ -403,7 +403,7 @@
     other = lax.ppermute(own, "core", swap)
     shared_far = shifted(shared_far, chips // 2, chips)
 
-    extra = up(up(slots, LANES) // LANES, 16)
+    extra = up(up(slots, LANES) // LANES, 8)
     weights = (w_gate[0].T, w_up[0].T)
     half = pltpu.VMEM((2 * units, width // 2), BF)
     give, dots, hidden, joined, x = local(
@@ -458,9 +458,9 @@
     )
 
     grad_shared, norm_shared = local(
-        shared_sum_kernel, (term_parts,), [((term.shape[1] * LANES // width, width), F32), ((1, LANES), F32)]
-    )
-    norm_shared = norm_shared[0, : grad_shared.shape[0]]
+        shared_sum_kernel, (term_parts,), [((term.shape[1] * LANES // width, width), F32), ((1, term.shape[1] * LANES // width), F32)]
+    )
+    norm_shared = norm_shared.reshape(-1)
     return (
         token_grad,
         gate_grad.T,

time: 141 us -> 140 us (level)
  transfers between devices with their start and end apart: 13 -> 13, of which waited for: 7 -> 7; matrix products, arithmetic and copies ran while one was open for 1% -> 0% of each run, Pallas kernels for 8% -> 8%
where the time goes in v3:
time: 140 us; the launch traced here: 138 us
  starting transfers between devices  73 us (52%)
  waiting for transfers between devices  46.4 us (33%)
  Pallas kernels  15 us (11%)
  local copies, waits for them, and re-layouts  2.66 us (2%)
    ppermute x5, starting transfers between devices, shifted(): return lax.ppermute(x, 'y', [(i, (i + by) % count) for i in range(count)])  21.7 us
    all_to_all x1, starting transfers between devices, all_steps(): lax.all_to_all(send.reshape(ep_count, 4 * cap, LANES), 'ep', 0, 0, tiled=...  18.8 us
    pallas_call x10, Pallas kernels, local(): pl.pallas_call(body, in_specs=specs, out_shape=tuple((jax.ShapeDtypeStruc...  12.6 us
    all_to_all x1, waiting for transfers between devices, all_steps(): lax.all_to_all(send.reshape(ep_count, 4 * cap, LANES), 'ep', 0, 0, tiled=...  11.2 us
    all_to_all x1, waiting for transfers between devices, all_steps(): pair_parts = lax.all_to_all(pair, 'y', 0, 0, tiled=True)  10.3 us
    all_to_all x1, waiting for transfers between devices, all_steps(): term_parts = lax.all_to_all(term, 'ep', 0, 0, tiled=True)  10.2 us
    all_to_all x1, starting transfers between devices, all_steps(): lax.all_to_all(back.reshape(ep_count, back_block, LANES), 'ep', 0, 0, til...  8.27 us
    ppermute x5, waiting for transfers between devices, shifted(): return lax.ppermute(x, 'y', [(i, (i + by) % count) for i in range(count)])  7.26 us
  transfers between devices with their start and end apart: 13, of which 7 were waited for; matrix products, arithmetic and copies ran while one was open for 0% of the time, Pallas kernels for 8%

profile of v3, /device:TPU:1, one launch (start us, length us, event | category | flops | bytes accessed | tf_op | source)
XLA Modules:
  0.0 137.9 jit_solution(11982832580908445521)
XLA Ops:
  0.6 0.0 copy-start
  0.7 0.0 copy-start.1
  0.7 0.0 copy-start.4
  0.7 2.4 %shard_map.169 = (bf16[1152,128]{1,0:T(8,128)(2,1)}, s32[2,128]{1,0:T(2,128)}) custom-call(s32[1]{0:T(128)} %bitcast.share_ref.at_ref, s32[2,128]{1,0:T(2,128)} %bitcast.27, f32[2,128]{1,0:T(2,128)} %bitcast.29, bf16[128,2048]{1,0:T(8,128)(2,1)} %tok_ref.1, bf16[128,2048]{1,0:T(8,128)(2,1)} %tok_ref.1, bf16[128,2048]{1,0:T(8,128)(2,1)} %cot_ref.1, ...), custom_call_target="tpu_custom_call" | custom-call | tf_op jit(solution)/shard_map/pallas_call | solution.py:357
  3.1 18.8 %all-to-all-start = ((bf16[48,24,128]{2,1,0:T(8,128)(2,1)}), bf16[48,24,128]{2,1,0:T(8,128)(2,1)S(1)}, u32[]{:S(2)}, u32[]{:S(2)}) async-start(bf16[48,24,128]{2,1,0:T(8,128)(2,1)} %bitcast.38), calls=%async_computation | async-start | bytes 589824 | tf_op jit(solution)/shard_map/all_to_all | solution.py:373
  22.0 2.3 %shard_map.170 = (bf16[8,128,128]{2,1,0:T(8,128)(2,1)S(1)}, bf16[8,128,128]{2,1,0:T(8,128)(2,1)S(1)}, bf16[48,32,128]{2,1,0:T(8,128)(2,1)}) custom-call(s32[1]{0:T(128)} %bitcast.share_ref.at_ref, bf16[128,2048]{1,0:T(8,128)(2,1)S(1)} %copy-done, bf16[128,2048]{1,0:T(8,128)(2,1)S(1)} %copy-done.1, bf16[96,2048]{1,0:T(8,128)(2,1)S(1)} %bitcast.31, ...), custom_call_target="tpu_custom_call" | custom-call | flops 4000000000 | bytes 8000000 | tf_op jit(solution)/shard_map/pallas_call | solution.py:327
  24.3 2.9 %collective-permute-start = (bf16[8,128,128]{2,1,0:T(8,128)(2,1)S(1)}, bf16[8,128,128]{2,1,0:T(8,128)(2,1)S(1)}, u32[]{:S(2)}, u32[]{:S(2)}) collective-permute-start(bf16[8,128,128]{2,1,0:T(8,128)(2,1)S(1)} %get-tuple-element.45), channel_id=1, source_target_pairs={{0,1},{1,0},{2,3},{3,2},{4,5},{5,4},{6,7},{7,6},{8,9},{9,8},{10,11... | collective-permute-start | bytes 786440 | tf_op jit(solution)/shard_map/ppermute | solution.py:384
  27.2 1.1 collective-permute-done.taken_ref
  28.3 11.2 %all-to-all-done = bf16[48,24,128]{2,1,0:T(8,128)(2,1)S(1)} async-done(((bf16[48,24,128]{2,1,0:T(8,128)(2,1)}), bf16[48,24,128]{2,1,0:T(8,128)(2,1)S(1)}, u32[]{:S(2)}, u32[]{:S(2)}) %all-to-all-start) | async-done | bytes 294944 | tf_op jit(solution)/shard_map/all_to_all | solution.py:373
  39.5 0.3 shard_map.171
  39.8 5.1 %collective-permute-start.2 = (bf16[1408,128]{1,0:T(8,128)(2,1)S(1)}, bf16[1408,128]{1,0:T(8,128)(2,1)S(1)}, u32[]{:S(2)}, u32[]{:S(2)}) collective-permute-start(bf16[1408,128]{1,0:T(8,128)(2,1)S(1)} %get-tuple-element.51), channel_id=1, source_target_pairs={{0,14},{2,0},{4,2},{6,4},{8,6},{10,8},{12,10},{14,12},{1,15},{3,1}... | collective-permute-start | bytes 1081352 | tf_op jit(solution)/shard_map/ppermute | solution.py:339
  45.0 1.9 %collective-permute-start.1 = (bf16[1408,128]{1,0:T(8,128)(2,1)S(1)}, bf16[1408,128]{1,0:T(8,128)(2,1)S(1)}, u32[]{:S(2)}, u32[]{:S(2)}) collective-permute-start(bf16[1408,128]{1,0:T(8,128)(2,1)S(1)} %get-tuple-element.50.mine_ref), channel_id=1, source_target_pairs={{0,2},{2,4},{4,6},{6,8},{8,10},{10,12},{12,14},{14,0},{1,3},{3,5},... | collective-permute-start | bytes 1081352 | tf_op jit(solution)/shard_map/ppermute | solution.py:339
  46.9 2.5 %collective-permute-start.3 = (bf16[704,128]{1,0:T(8,128)(2,1)S(1)}, bf16[704,128]{1,0:T(8,128)(2,1)S(1)}, u32[]{:S(2)}, u32[]{:S(2)}) collective-permute-start(bf16[704,128]{1,0:T(8,128)(2,1)S(1)} %get-tuple-element.52), channel_id=1, source_target_pairs={{0,4},{2,6},{4,8},{6,10},{8,12},{10,14},{12,0},{14,2},{1,5},{3,7},... | collective-permute-start | bytes 540680 | tf_op jit(solution)/shard_map/ppermute | solution.py:339
  49.4 4.9 %collective-permute-start.4 = (bf16[704,128]{1,0:T(8,128)(2,1)S(1)}, bf16[704,128]{1,0:T(8,128)(2,1)S(1)}, u32[]{:S(2)}, u32[]{:S(2)}) collective-permute-start(bf16[704,128]{1,0:T(8,128)(2,1)S(1)} %get-tuple-element.53), channel_id=1, source_target_pairs={{0,12},{2,14},{4,0},{6,2},{8,4},{10,6},{12,8},{14,10},{1,13},{3,15... | collective-permute-start | bytes 540680 | tf_op jit(solution)/shard_map/ppermute | solution.py:339
  54.3 6.1 %collective-permute-done.3.far_up_ref = bf16[704,128]{1,0:T(8,128)(2,1)S(1)} collective-permute-done((bf16[704,128]{1,0:T(8,128)(2,1)S(1)}, bf16[704,128]{1,0:T(8,128)(2,1)S(1)}, u32[]{:S(2)}, u32[]{:S(2)}) %collective-permute-start.3) | collective-permute-done | bytes 180256 | tf_op jit(solution)/shard_map/ppermute | solution.py:339
  60.4 1.2 collective-permute-done.4.far_down_ref
  61.5 0.0 collective-permute-done.2.down_ref
  61.5 0.0 collective-permute-done.1.up_ref
  61.6 0.1 shard_map.172
  61.7 5.5 %collective-permute-start.5 = (bf16[8,576,128]{2,1,0:T(8,128)(2,1)S(1)}, bf16[8,576,128]{2,1,0:T(8,128)(2,1)S(1)}, u32[]{:S(2)}, u32[]{:S(2)}) collective-permute-start(bf16[8,576,128]{2,1,0:T(8,128)(2,1)S(1)} %get-tuple-element.55.own_ref), channel_id=1, source_target_pairs={{0,1},{1,0},{2,3},{3,2},{4,5},{5,4},{6,7},{7,6},{8,9},{9,8},{10,11... | collective-permute-start | bytes 3538952 | tf_op jit(solution)/shard_map/ppermute | solution.py:403
  67.2 5.1 %all-to-all-start.3 = ((bf16[48,32,128]{2,1,0:T(8,128)(2,1)}), bf16[48,32,128]{2,1,0:T(8,128)(2,1)S(1)}, u32[]{:S(2)}, u32[]{:S(2)}) async-start(bf16[48,32,128]{2,1,0:T(8,128)(2,1)} %get-tuple-element.72), calls=%async_computation.3 | async-start | bytes 786432 | tf_op jit(solution)/shard_map/all_to_all | solution.py:386
  72.3 0.0 collective-permute-done.5.other_ref
  72.3 0.0 copy-start.8
  72.3 1.0 copy-done.8
  73.3 1.0 copy-done.10
  74.3 2.5 %shard_map.173 = (bf16[8,296,128]{2,1,0:T(8,128)(2,1)S(1)}, bf16[8,128]{1,0:T(8,128)(2,1)S(1)}, bf16[96,288]{1,0:T(8,128)(2,1)S(1)}, bf16[192,288]{1,0:T(8,128)(2,1)S(1)}, bf16[288,2048]{1,0:T(8,128)(2,1)S(1)}) custom-call(s32[1]{0:T(128)} %bitcast.share_ref.at_ref, bf16[8,576,128]{2,1,0:T(8,128)(2,1)S(1)} %get-tuple-element.55.own_ref, ...), custom_call_target="tpu_custom_call" | custom-call | flops 6000000000 | bytes 12000000 | tf_op jit(solution)/shard_map/pallas_call | solution.py:327
  76.9 2.2 %collective-permute-start.6 = (bf16[8,296,128]{2,1,0:T(8,128)(2,1)S(1)}, bf16[8,296,128]{2,1,0:T(8,128)(2,1)S(1)}, u32[]{:S(2)}, u32[]{:S(2)}) collective-permute-start(bf16[8,296,128]{2,1,0:T(8,128)(2,1)S(1)} %get-tuple-element.59), channel_id=1, source_target_pairs={{0,1},{1,0},{2,3},{3,2},{4,5},{5,4},{6,7},{7,6},{8,9},{9,8},{10,11... | collective-permute-start | bytes 1818632 | tf_op jit(solution)/shard_map/ppermute | solution.py:423
  79.1 2.0 %shard_map.174 = (bf16[8,288,128]{2,1,0:T(8,128)(2,1)S(1)}, f32[96,2048]{1,0:T(8,128)}, f32[96,2048]{1,0:T(8,128)}, bf16[32,128]{1,0:T(8,128)(2,1)S(1)}) custom-call(s32[1]{0:T(128)} %bitcast.share_ref.at_ref, bf16[288,2048]{1,0:T(8,128)(2,1)S(1)} %get-tuple-element.56.x_ref, bf16[192,288]{1,0:T(8,128)(2,1)S(1)} %get-tuple-element.57.joined_ref, ...), custom_call_target="tpu_custom_call" | custom-call | flops 4000000000 | bytes 8000000 | tf_op jit(solution)/shard_map/pallas_call | solution.py:327
  81.0 0.0 collective-permute-done.6.taken_ref
  81.0 1.0 shard_map.175
  82.0 10.2 %all-to-all-done.3.parts_ref = bf16[48,32,128]{2,1,0:T(8,128)(2,1)S(1)} async-done(((bf16[48,32,128]{2,1,0:T(8,128)(2,1)}), bf16[48,32,128]{2,1,0:T(8,128)(2,1)S(1)}, u32[]{:S(2)}, u32[]{:S(2)}) %all-to-all-start.3) | async-done | bytes 393248 | tf_op jit(solution)/shard_map/all_to_all | solution.py:386
  92.2 5.7 %all-to-all-start.1 = ((bf16[8,328,128]{2,1,0:T(8,128)(2,1)}), bf16[8,328,128]{2,1,0:T(8,128)(2,1)S(1)}, u32[]{:S(2)}, u32[]{:S(2)}) async-start(bf16[8,328,128]{2,1,0:T(8,128)(2,1)} %shard_map.175), calls=%async_computation.1 | async-start | bytes 1343488 | tf_op jit(solution)/shard_map/all_to_all | solution.py:436
  98.0 7.3 %collective-permute-start.7 = (bf16[128,128]{1,0:T(8,128)(2,1)S(1)}, bf16[128,128]{1,0:T(8,128)(2,1)S(1)}, u32[]{:S(2)}, u32[]{:S(2)}) collective-permute-start(bf16[128,128]{1,0:T(8,128)(2,1)S(1)} %get-tuple-element.65), channel_id=1, source_target_pairs={{0,8},{2,10},{4,12},{6,14},{8,0},{10,2},{12,4},{14,6},{1,9},{3,11}... | collective-permute-start | bytes 98312 | tf_op jit(solution)/shard_map/ppermute | solution.py:339
  105.2 0.7 shard_map.179
  105.9 10.3 %all-to-all-done.1.parts_ref = bf16[8,328,128]{2,1,0:T(8,128)(2,1)S(1)} async-done(((bf16[8,328,128]{2,1,0:T(8,128)(2,1)}), bf16[8,328,128]{2,1,0:T(8,128)(2,1)S(1)}, u32[]{:S(2)}, u32[]{:S(2)}) %all-to-all-start.1) | async-done | bytes 671776 | tf_op jit(solution)/shard_map/all_to_all | solution.py:436
  116.3 1.1 shard_map.176
  117.4 8.3 %all-to-all-start.2 = ((bf16[48,8,128]{2,1,0:T(8,128)(2,1)}), bf16[48,8,128]{2,1,0:T(8,128)(2,1)S(1)}, u32[]{:S(2)}, u32[]{:S(2)}) async-start(bf16[48,8,128]{2,1,0:T(8,128)(2,1)} %bitcast.12), calls=%async_computation.2 | async-start | bytes 196608 | tf_op jit(solution)/shard_map/all_to_all | solution.py:453
  125.7 2.8 %collective-permute-start.8 = (f32[32,128]{1,0:T(8,128)S(1)}, f32[32,128]{1,0:T(8,128)S(1)}, u32[]{:S(2)}, u32[]{:S(2)}) collective-permute-start(f32[32,128]{1,0:T(8,128)S(1)} %get-tuple-element.74), channel_id=1, source_target_pairs={{0,1},{1,0},{2,3},{3,2},{4,5},{5,4},{6,7},{7,6},{8,9},{9,8},{10,11... | collective-permute-start | bytes 49160 | tf_op jit(solution)/shard_map/ppermute | solution.py:451
  128.5 0.0 copy-start.2
  128.5 0.0 copy-start.3
  128.5 0.0 copy-start.11
  128.5 1.7 %shard_map.178 = (f32[96,2048]{1,0:T(8,128)}, f32[1,96]{1,0:T(1,128)}) custom-call(s32[1]{0:T(128)} %bitcast.share_ref.at_ref, bf16[8,576,128]{2,1,0:T(8,128)(2,1)S(1)} %get-tuple-element.55.own_ref, bf16[8,576,128]{2,1,0:T(8,128)(2,1)S(1)} %collective-permute-done.5.other_ref, bf16[96,288]{1,0:T(8,128)(2,1)S(1)} %copy-done.13), custom_call_target="tpu_custom_call" | custom-call | flops 3000000000 | bytes 6000000 | tf_op jit(solution)/shard_map/pallas_call | solution.py:327
  130.2 0.0 collective-permute-done.8
  130.2 0.6 broadcast_in_dim_reshape.3
  130.8 0.0 collective-permute-done.7.far_ref
  130.8 6.2 %all-to-all-done.2 = bf16[48,8,128]{2,1,0:T(8,128)(2,1)S(1)} async-done(((bf16[48,8,128]{2,1,0:T(8,128)(2,1)}), bf16[48,8,128]{2,1,0:T(8,128)(2,1)S(1)}, u32[]{:S(2)}, u32[]{:S(2)}) %all-to-all-start.2) | async-done | bytes 98336 | tf_op jit(solution)/shard_map/all_to_all | solution.py:453
  137.0 0.0 copy-done.3
  137.1 0.9 shard_map.177
  (19 shorter events, 0.0 us)
Async XLA Ops:
  0.6 21.3 %copy-start = (bf16[128,2048]{1,0:T(8,128)(2,1)S(1)}, bf16[128,2048]{1,0:T(8,128)(2,1)}, u32[]{:S(2)}) copy-start(bf16[128,2048]{1,0:T(8,128)(2,1)} %tok_ref.1) | copy-start | bytes 1572868
  0.7 21.3 %copy-start.1 = (bf16[128,2048]{1,0:T(8,128)(2,1)S(1)}, bf16[128,2048]{1,0:T(8,128)(2,1)}, u32[]{:S(2)}) copy-start(bf16[128,2048]{1,0:T(8,128)(2,1)} %cot_ref.1) | copy-start | bytes 1572868
  0.7 21.3 %copy-start.4 = (bf16[2048,96]{0,1:T(8,128)(2,1)S(1)}, bf16[2048,96]{0,1:T(8,128)(2,1)}, u32[]{:S(2)}) copy-start(bf16[2048,96]{0,1:T(8,128)(2,1)} %param.17) | copy-start | bytes 1179652
  0.7 21.3 %copy-start.5 = (bf16[2048,96]{0,1:T(8,128)(2,1)S(1)}, bf16[2048,96]{0,1:T(8,128)(2,1)}, u32[]{:S(2)}) copy-start(bf16[2048,96]{0,1:T(8,128)(2,1)} %param.18) | copy-start | bytes 1179652
  0.7 21.3 %copy-start.6 = (bf16[96,2048]{1,0:T(8,128)(2,1)S(1)}, bf16[96,2048]{1,0:T(8,128)(2,1)}, u32[]{:S(2)}) copy-start(bf16[96,2048]{1,0:T(8,128)(2,1)} %down_ref.1) | copy-start | bytes 1179652
  3.1 36.4 %all-to-all-start = ((bf16[48,24,128]{2,1,0:T(8,128)(2,1)}), bf16[48,24,128]{2,1,0:T(8,128)(2,1)S(1)}, u32[]{:S(2)}, u32[]{:S(2)}) async-start(bf16[48,24,128]{2,1,0:T(8,128)(2,1)} %bitcast.38), calls=%async_computation | async-start | bytes 589824 | tf_op jit(solution)/shard_map/all_to_all | solution.py:373
  24.3 4.0 %collective-permute-start = (bf16[8,128,128]{2,1,0:T(8,128)(2,1)S(1)}, bf16[8,128,128]{2,1,0:T(8,128)(2,1)S(1)}, u32[]{:S(2)}, u32[]{:S(2)}) collective-permute-start(bf16[8,128,128]{2,1,0:T(8,128)(2,1)S(1)} %get-tuple-element.45), channel_id=1, source_target_pairs={{0,1},{1,0},{2,3},{3,2},{4,5},{5,4},{6,7},{7,6},{8,9},{9,8},{10,11... | collective-permute-start | bytes 786440 | tf_op jit(solution)/shard_map/ppermute | solution.py:384
  39.8 21.7 %collective-permute-start.2 = (bf16[1408,128]{1,0:T(8,128)(2,1)S(1)}, bf16[1408,128]{1,0:T(8,128)(2,1)S(1)}, u32[]{:S(2)}, u32[]{:S(2)}) collective-permute-start(bf16[1408,128]{1,0:T(8,128)(2,1)S(1)} %get-tuple-element.51), channel_id=1, source_target_pairs={{0,14},{2,0},{4,2},{6,4},{8,6},{10,8},{12,10},{14,12},{1,15},{3,1}... | collective-permute-start | bytes 1081352 | tf_op jit(solution)/shard_map/ppermute | solution.py:339
  45.0 16.6 %collective-permute-start.1 = (bf16[1408,128]{1,0:T(8,128)(2,1)S(1)}, bf16[1408,128]{1,0:T(8,128)(2,1)S(1)}, u32[]{:S(2)}, u32[]{:S(2)}) collective-permute-start(bf16[1408,128]{1,0:T(8,128)(2,1)S(1)} %get-tuple-element.50.mine_ref), channel_id=1, source_target_pairs={{0,2},{2,4},{4,6},{6,8},{8,10},{10,12},{12,14},{14,0},{1,3},{3,5},... | collective-permute-start | bytes 1081352 | tf_op jit(solution)/shard_map/ppermute | solution.py:339
  46.9 13.5 %collective-permute-start.3 = (bf16[704,128]{1,0:T(8,128)(2,1)S(1)}, bf16[704,128]{1,0:T(8,128)(2,1)S(1)}, u32[]{:S(2)}, u32[]{:S(2)}) collective-permute-start(bf16[704,128]{1,0:T(8,128)(2,1)S(1)} %get-tuple-element.52), channel_id=1, source_target_pairs={{0,4},{2,6},{4,8},{6,10},{8,12},{10,14},{12,0},{14,2},{1,5},{3,7},... | collective-permute-start | bytes 540680 | tf_op jit(solution)/shard_map/ppermute | solution.py:339
  49.4 12.2 %collective-permute-start.4 = (bf16[704,128]{1,0:T(8,128)(2,1)S(1)}, bf16[704,128]{1,0:T(8,128)(2,1)S(1)}, u32[]{:S(2)}, u32[]{:S(2)}) collective-permute-start(bf16[704,128]{1,0:T(8,128)(2,1)S(1)} %get-tuple-element.53), channel_id=1, source_target_pairs={{0,12},{2,14},{4,0},{6,2},{8,4},{10,6},{12,8},{14,10},{1,13},{3,15... | collective-permute-start | bytes 540680 | tf_op jit(solution)/shard_map/ppermute | solution.py:339
  61.5 10.8 %copy-start.7 = (bf16[1,96,2048]{2,1,0:T(8,128)(2,1)S(1)}, bf16[1,96,2048]{2,1,0:T(8,128)(2,1)}, u32[]{:S(2)}) copy-start(bf16[1,96,2048]{2,1,0:T(8,128)(2,1)} %param.16) | copy-start | bytes 1179652
  61.7 10.6 %collective-permute-start.5 = (bf16[8,576,128]{2,1,0:T(8,128)(2,1)S(1)}, bf16[8,576,128]{2,1,0:T(8,128)(2,1)S(1)}, u32[]{:S(2)}, u32[]{:S(2)}) collective-permute-start(bf16[8,576,128]{2,1,0:T(8,128)(2,1)S(1)} %get-tuple-element.55.own_ref), channel_id=1, source_target_pairs={{0,1},{1,0},{2,3},{3,2},{4,5},{5,4},{6,7},{7,6},{8,9},{9,8},{10,11... | collective-permute-start | bytes 3538952 | tf_op jit(solution)/shard_map/ppermute | solution.py:403
  67.2 25.0 %all-to-all-start.3 = ((bf16[48,32,128]{2,1,0:T(8,128)(2,1)}), bf16[48,32,128]{2,1,0:T(8,128)(2,1)S(1)}, u32[]{:S(2)}, u32[]{:S(2)}) async-start(bf16[48,32,128]{2,1,0:T(8,128)(2,1)} %get-tuple-element.72), calls=%async_computation.3 | async-start | bytes 786432 | tf_op jit(solution)/shard_map/all_to_all | solution.py:386
  72.3 1.0 copy-start.8
  73.3 1.0 copy-start.10
  74.3 4.8 %copy-start.9 = (bf16[1,2048,96]{1,2,0:T(8,128)(2,1)S(1)}, bf16[1,2048,96]{1,2,0:T(8,128)(2,1)}, u32[]{:S(2)}) copy-start(bf16[1,2048,96]{1,2,0:T(8,128)(2,1)} %param.14) | copy-start | bytes 1179652
  76.9 4.2 %copy-start.12 = (bf16[96,288]{1,0:T(8,128)(2,1)}, bf16[96,288]{1,0:T(8,128)(2,1)S(1)}, u32[]{:S(2)}) copy-start(bf16[96,288]{1,0:T(8,128)(2,1)S(1)} %get-tuple-element.70.hidden_ref) | copy-start | bytes 165892
  76.9 4.2 %collective-permute-start.6 = (bf16[8,296,128]{2,1,0:T(8,128)(2,1)S(1)}, bf16[8,296,128]{2,1,0:T(8,128)(2,1)S(1)}, u32[]{:S(2)}, u32[]{:S(2)}) collective-permute-start(bf16[8,296,128]{2,1,0:T(8,128)(2,1)S(1)} %get-tuple-element.59), channel_id=1, source_target_pairs={{0,1},{1,0},{2,3},{3,2},{4,5},{5,4},{6,7},{7,6},{8,9},{9,8},{10,11... | collective-permute-start | bytes 1818632 | tf_op jit(solution)/shard_map/ppermute | solution.py:423
  92.2 24.0 %all-to-all-start.1 = ((bf16[8,328,128]{2,1,0:T(8,128)(2,1)}), bf16[8,328,128]{2,1,0:T(8,128)(2,1)S(1)}, u32[]{:S(2)}, u32[]{:S(2)}) async-start(bf16[8,328,128]{2,1,0:T(8,128)(2,1)} %shard_map.175), calls=%async_computation.1 | async-start | bytes 1343488 | tf_op jit(solution)/shard_map/all_to_all | solution.py:436
  98.0 32.9 %collective-permute-start.7 = (bf16[128,128]{1,0:T(8,128)(2,1)S(1)}, bf16[128,128]{1,0:T(8,128)(2,1)S(1)}, u32[]{:S(2)}, u32[]{:S(2)}) collective-permute-start(bf16[128,128]{1,0:T(8,128)(2,1)S(1)} %get-tuple-element.65), channel_id=1, source_target_pairs={{0,8},{2,10},{4,12},{6,14},{8,0},{10,2},{12,4},{14,6},{1,9},{3,11}... | collective-permute-start | bytes 98312 | tf_op jit(solution)/shard_map/ppermute | solution.py:339
  105.9 22.6 %copy-start.13 = (bf16[96,288]{1,0:T(8,128)(2,1)S(1)}, bf16[96,288]{1,0:T(8,128)(2,1)}, u32[]{:S(2)}) copy-start(bf16[96,288]{1,0:T(8,128)(2,1)} %copy-done.12) | copy-start | bytes 165892
  117.4 19.7 %all-to-all-start.2 = ((bf16[48,8,128]{2,1,0:T(8,128)(2,1)}), bf16[48,8,128]{2,1,0:T(8,128)(2,1)S(1)}, u32[]{:S(2)}, u32[]{:S(2)}) async-start(bf16[48,8,128]{2,1,0:T(8,128)(2,1)} %bitcast.12), calls=%async_computation.2 | async-start | bytes 196608 | tf_op jit(solution)/shard_map/all_to_all | solution.py:453
  125.7 4.5 %collective-permute-start.8 = (f32[32,128]{1,0:T(8,128)S(1)}, f32[32,128]{1,0:T(8,128)S(1)}, u32[]{:S(2)}, u32[]{:S(2)}) collective-permute-start(f32[32,128]{1,0:T(8,128)S(1)} %get-tuple-element.74), channel_id=1, source_target_pairs={{0,1},{1,0},{2,3},{3,2},{4,5},{5,4},{6,7},{7,6},{8,9},{9,8},{10,11... | collective-permute-start | bytes 49160 | tf_op jit(solution)/shard_map/ppermute | solution.py:451
  128.5 8.6 %copy-start.2 = (s32[128,2]{0,1:T(2,128)S(1)}, s32[128,2]{0,1:T(2,128)}, u32[]{:S(2)}) copy-start(s32[128,2]{0,1:T(2,128)} %param.11) | copy-start | bytes 3076
  128.5 8.5 %copy-start.3 = (f32[128,2]{0,1:T(2,128)S(1)}, f32[128,2]{0,1:T(2,128)}, u32[]{:S(2)}) copy-start(f32[128,2]{0,1:T(2,128)} %param.12) | copy-start | bytes 3076
  128.5 8.5 %copy-start.11 = (s32[2,128]{1,0:T(2,128)S(1)}, s32[2,128]{1,0:T(2,128)}, u32[]{:S(2)}) copy-start(s32[2,128]{1,0:T(2,128)} %get-tuple-element.63.rank_ref) | copy-start | bytes 3076
